TPU v7x, 128 devices: a whole 4x4x4 slice. The times are simulated.
128 devices in a mesh: sp: 64 (over z, y, x), tp: 2 (over core).
Axes of the slice: x: 4, y: 4, z: 4, core: 2. Of those that a mesh axis runs over, the one named last changes fastest.
Arguments:
- wide_inputs: bfloat16 [8192, 512], P('sp', 'tp'), may hold values from -6 to 6
- narrow_inputs: bfloat16 [8192, 512], P('sp', 'tp'), may hold values from -6 to 6
- wide_poles: float32 [2, 2, 32, 64], P(None, None, 'tp'), may hold values from -3.1416 to 3.1416, as said below
- narrow_poles: float32 [2, 2, 32, 32], P(None, None, 'tp'), may hold values from -3.1416 to 3.1416, as said below
- step_sizes: float32 [2, 2, 32], P(None, None, 'tp'), may hold values from 0 to 1, as said below
- forget: float32 [2, 2, 32, 8192], P(None, None, 'tp', 'sp'), may hold values from 0 to 2.2
- wide_in_map: float32 [2, 2, 32, 16, 64], P(None, None, 'tp'), may hold values from -2.5 to 2.5
- narrow_in_map: float32 [2, 2, 32, 16, 32], P(None, None, 'tp'), may hold values from -2.5 to 2.5
- wide_out_map: float32 [2, 2, 32, 16, 64], P(None, None, 'tp'), may hold values from -1.25 to 1.25
- narrow_out_map: float32 [2, 2, 32, 16, 32], P(None, None, 'tp'), may hold values from -2 to 2
- skip_weight: bfloat16 [2, 512], P(None, 'tp'), may hold values from -6 to 6
- gate_mix: bfloat16 [2, 32, 16, 16], P(None, 'tp'), may hold values from -1.5 to 1.5
- residual: bfloat16 [8192, 2048], P(('sp', 'tp')), may hold values from -6 to 6
- mixer_gain: float32 [1024], replicated, may hold values from 0.1 to 1.9
- out_proj: bfloat16 [1024, 2048], replicated, may hold values from -0.1875 to 0.1875
- ffn_gain: float32 [2048], replicated, may hold values from 0.1 to 1.9
- routes: int32 [8192, 2], P(('sp', 'tp')), may hold values from 0 to 127, all different within a row; in each aligned block of 64 rows (0 to 63, 64 to 127, ...) at most 2 rows name the same one
- route_weights: float32 [8192, 2], P(('sp', 'tp')), may hold values from 0.1 to 1
- gate_proj: bfloat16 [128, 2048, 1408], P(('sp', 'tp')), may hold values from -0.125 to 0.125
- up_proj: bfloat16 [128, 2048, 1408], P(('sp', 'tp')), may hold values from -0.125 to 0.125
- down_proj: bfloat16 [128, 1408, 2048], P(('sp', 'tp')), may hold values from -0.15625 to 0.15625
Outputs:
- layer_out: bfloat16 [8192, 2048], P(('sp', 'tp'))
Inputs may be any that keep to these rules, and one draw needn't show every extreme that they name: `routes`: in each aligned block of 64 rows (the rows of one device), no expert is named by more than 2 entries, and the 2 experts of a row differ. `wide_poles`: along dimension 1, entry 0 (the real part) is negative and entry 1 (the imaginary part) is at least 0.1 in magnitude. `narrow_poles`: along dimension 1, entry 0 (the real part) is negative and entry 1 (the imaginary part) is at least 0.1 in magnitude. `step_sizes`: Positive.
All inputs are finite; a program needn't handle non-finite values.
Results may differ from a plain program's by a relative error of at most 0.014.
Values may be sent and summed in bfloat16 or wider, within the bound.
No kernel may reach another device: no remote copies, remote signals or barrier semaphores. Data moves between devices by JAX's collectives and lax.ppermute only.
A program may use at most 192 MiB of HBM per device.

v0:
```python
import functools

import jax
import jax.numpy as jnp
from jax import lax
from jax.experimental import pallas as pl
from jax.experimental.pallas import tpu as pltpu
from jax.sharding import Mesh
from jax.sharding import PartitionSpec as P

SP = ("sp_0", "sp_1", "sp_2")
SP_TP = ("sp_0", "sp_1", "sp_2", "tp")
EPS = 1e-06
F32 = jnp.float32
BF16 = jnp.bfloat16
T = 128
LANES = 128
NT = (((1,), (1,)), ((), ()))
WIDE = (8, 2, 64)
NARROW = (4, 4, 32)


def lane_ids(shape):
    return lax.broadcasted_iota(jnp.int32, shape, len(shape) - 1)


def in_rows(grouped, kind):
    rows, parts, _ = kind
    return jnp.concatenate([grouped[rows * h : rows * (h + 1)] for h in range(parts)], axis=1)


def side_by_side(pieces, row, kind):
    rows, parts, _ = kind
    return jnp.concatenate([pieces[row + rows * h] for h in range(parts)], axis=1)


def padded8(rows):
    if rows.shape[0] == 8:
        return rows
    return jnp.concatenate([rows, jnp.zeros((8 - rows.shape[0], LANES), F32)], axis=0)


def discretized(poles_ref, d):
    pr, pi = poles_ref[d, 0], poles_ref[d, 1]
    growth = jnp.exp(pr)
    cr, ci = growth * jnp.cos(pi), growth * jnp.sin(pi)
    nr = cr - 1.0
    denom = pr * pr + pi * pi
    fr = (nr * pr + ci * pi) / denom
    fi = (ci * pr - nr * pi) / denom
    return cr, ci, fr, fi


def group_block(row, r, kind):
    rows, parts, states = kind
    ids = (lane_ids(row.shape) % LANES) // states
    zeros = lambda n: [jnp.zeros((n, 2 * LANES), BF16)] if n else []
    row = row.astype(F32)
    out, at = [], 0
    for h in range(parts):
        start = 16 * (r + rows * h)
        out += zeros(start - at) + [jnp.where(ids == h, row, 0.0).astype(BF16)]
        at = start + 16
    return jnp.concatenate(out + zeros(16 * 16 - at), axis=0)


def spread(table, base, r, kind):
    rows, parts, states = kind
    n = table.shape[0]
    lanes = lane_ids((n, LANES)) // states
    out = jnp.broadcast_to(table[:, base + r : base + r + 1], (n, LANES))
    for h in range(1, parts):
        k = base + r + rows * h
        out = jnp.where(lanes == h, jnp.broadcast_to(table[:, k : k + 1], (n, LANES)), out)
    return out


def push_into(steps_ref, which, d, u, poles_ref, in_ref, kind, re_ref, im_ref):
    rows, parts, _ = kind
    cr, ci, fr, fi = discretized(poles_ref, d)
    for r in range(rows):
        re, im = [], []
        for h in range(parts):
            g = r + rows * h
            step = steps_ref[(d * 2 + which) * 16 + g]
            gr, gi = fr[g : g + 1] * step, fi[g : g + 1] * step
            br, bi = in_ref[d, 0, g], in_ref[d, 1, g]
            re.append(gr * br - gi * bi)
            im.append(gr * bi + gi * br)
        row = jnp.concatenate([jnp.concatenate(re, axis=1), jnp.concatenate(im, axis=1)], axis=1)
        driven = jnp.dot(u, group_block(row, r, kind), preferred_element_type=F32)
        re_ref[pl.ds(r, T, stride=8), :] = driven[:, :LANES]
        im_ref[pl.ds(r, T, stride=8), :] = driven[:, LANES:]
    return padded8(in_rows(cr, kind)), padded8(in_rows(ci, kind))


def forget_columns(forget_ref):
    both = forget_ref[...]
    return jnp.transpose(jnp.concatenate([both, both], axis=0))


def load_pushes(steps_ref, u_refs, pole_refs, in_refs, forget_t, scr):
    kept = jnp.exp(-forget_t)
    turns = []
    for d in range(2):
        for which, kind in ((0, WIDE), (1, NARROW)):
            re_ref, im_ref, e_ref = scr[(d * 2 + which) * 3 : (d * 2 + which) * 3 + 3]
            if kind is NARROW:
                for ref in (re_ref, im_ref, e_ref):
                    ref[...] = jnp.zeros((8 * T, LANES), F32)
            for r in range(kind[0]):
                e_ref[pl.ds(r, T, stride=8), :] = spread(kept, (d * 2 + which) * 16, r, kind)
            turns.append(
                push_into(
                    steps_ref, which, d, u_refs[which][...], pole_refs[which], in_refs[which],
                    kind, re_ref, im_ref,
                )
            )
    return turns


def three_terms(x):
    hi = x.astype(BF16).astype(F32)
    mid = (x - hi).astype(BF16).astype(F32)
    return hi, mid, x - hi - mid


def ends_kernel(
    me_ref, steps_ref, wu_ref, nu_ref, wp_ref, np_ref, wi_ref, ni_ref, forget_ref, send_ref, *scr
):
    forget_t = forget_columns(forget_ref)
    turns = load_pushes(
        steps_ref, (wu_ref, nu_ref), (wp_ref, np_ref), (wi_ref, ni_ref), forget_t, scr
    )

    def step(t, state):
        new = []
        for k in range(4):
            re_ref, im_ref, e_ref = scr[3 * k : 3 * k + 3]
            at = pl.multiple_of((t if k < 2 else T - 1 - t) * 8, 8)
            (cr, ci), (sr, si) = turns[k], state[k]
            e = e_ref[pl.ds(at, 8), :]
            new.append(
                (
                    e * (cr * sr - ci * si) + re_ref[pl.ds(at, 8), :],
                    e * (cr * si + ci * sr) + im_ref[pl.ds(at, 8), :],
                )
            )
        return tuple(new)

    zero = jnp.zeros((8, LANES), F32)
    state = lax.fori_loop(0, T, step, ((zero, zero),) * 4, unroll=8)
    kept = jnp.exp(-jnp.sum(forget_t, axis=0, keepdims=True))
    hi, mid, lo = three_terms(kept)
    first = lane_ids((1, LANES)) < 64
    terms = jnp.where(first, hi, mid)
    rest = jnp.where(first, lo, 0.0)
    row = lax.broadcasted_iota(jnp.int32, (8, LANES), 0)
    blocks = []
    for d in range(2):
        (wr, wi), (nr, ni) = state[2 * d], state[2 * d + 1]
        nr = jnp.where(row < 4, nr, jnp.where(row == 4, terms, jnp.where(row == 5, rest, 0.0)))
        blocks.append(jnp.concatenate([wr, wi, nr, jnp.where(row < 4, ni, 0.0)], axis=0))
    me = me_ref[0]

    def put(j, _):
        at = pl.multiple_of(j * 32, 32)
        send_ref[pl.ds(at, 32), :] = jnp.where(j > me, blocks[0], blocks[1]).astype(BF16)
        return 0

    lax.fori_loop(0, send_ref.shape[0] // 32, put, 0)


def read_blocks(out_ref, d, r, kind):
    return side_by_side(out_ref[d, 0], r, kind), side_by_side(out_ref[d, 1], r, kind)


def local_kernel(
    steps_ref, wu_ref, nu_ref, wp_ref, np_ref, wi_ref, ni_ref, forget_ref, wo_ref, no_ref, after_ref,
    y_ref, decay_ref, *scr
):
    del after_ref
    turns = load_pushes(
        steps_ref, (wu_ref, nu_ref), (wp_ref, np_ref), (wi_ref, ni_ref),
        forget_columns(forget_ref), scr,
    )
    prods = scr[12:]

    def step(t, state):
        new = []
        for k in range(4):
            re_ref, im_ref, e_ref = scr[3 * k : 3 * k + 3]
            at = pl.ds(pl.multiple_of((t if k < 2 else T - 1 - t) * 8, 8), 8)
            (cr, ci), (sr, si, pr, pi) = turns[k], state[k]
            e = e_ref[at, :]
            got = (
                e * (cr * sr - ci * si) + re_ref[at, :],
                e * (cr * si + ci * sr) + im_ref[at, :],
                e * (cr * pr - ci * pi),
                e * (cr * pi + ci * pr),
            )
            re_ref[at, :], im_ref[at, :] = got[0], got[1]
            prods[2 * k][at, :], prods[2 * k + 1][at, :] = got[2], got[3]
            new.append(got)
        return tuple(new)

    zero = jnp.zeros((8, LANES), F32)
    lax.fori_loop(0, T, step, ((zero, zero, zero + 1.0, zero),) * 4, unroll=4)
    for which, (kind, out_ref) in enumerate(((WIDE, wo_ref), (NARROW, no_ref))):
        total = jnp.zeros((T, 2 * LANES), F32)
        for d in range(2):
            k = d * 2 + which
            for r in range(kind[0]):
                at = pl.ds(r, T, stride=8)
                o_re, o_im = read_blocks(out_ref, d, r, kind)
                weights = group_block(jnp.concatenate([o_re, -o_im], axis=1), r, kind)
                hidden = jnp.concatenate([scr[3 * k][at, :], scr[3 * k + 1][at, :]], axis=1)
                total += lax.dot_general(
                    hidden.astype(BF16), weights, NT, preferred_element_type=F32
                )
                decay = jnp.concatenate([prods[2 * k][at, :], prods[2 * k + 1][at, :]], axis=1)
                first = ((d * 12) + which * 8 + r) * 2 * LANES
                decay_ref[:, first : first + 2 * LANES] = decay.astype(BF16)
        y_ref[:, which * 2 * LANES : (which + 1) * 2 * LANES] = total


def carry_kernel(
    me_ref, got_ref, wu_ref, nu_ref, wp_ref, np_ref, wo_ref, no_ref, y_ref, decay_ref, skip_ref,
    gate_ref, out_ref, flat, *kept
):
    me = me_ref[0]
    blocks = got_ref.shape[0] // 32
    flat[...] = got_ref[...].astype(F32)
    first = flat[pl.ds(20, blocks, stride=32), :]
    table = first + pltpu.roll(first, 64, 1) + flat[pl.ds(21, blocks, stride=32), :]
    turns = []
    for d in range(2):
        for which, (kind, poles_ref) in enumerate(((WIDE, wp_ref), (NARROW, np_ref))):
            k = d * 2 + which
            if kind is NARROW:
                kept[k][...] = jnp.zeros((8 * blocks, LANES), F32)
            for r in range(kind[0]):
                kept[k][pl.ds(r, blocks, stride=8), :] = spread(table, k * 16, r, kind)
            pr, pi = poles_ref[d, 0], poles_ref[d, 1]
            growth = jnp.exp(pr)
            cr, ci = growth * jnp.cos(pi), growth * jnp.sin(pi)
            for _ in range(7):
                cr, ci = cr * cr - ci * ci, 2.0 * cr * ci
            turns.append((padded8(in_rows(cr, kind)), padded8(in_rows(ci, kind))))

    def step(i, state):
        new = []
        for k in range(4):
            j = i if k < 2 else blocks - 1 - i
            used = (j < me) if k < 2 else (j > me)
            base = pl.multiple_of(j * 32, 32)
            re_at, im_at = (0, 8) if k % 2 == 0 else (16, 24)
            (cr, ci), (sr, si) = turns[k], state[k]
            e = kept[k][pl.ds(pl.multiple_of(j * 8, 8), 8), :]
            re = e * (cr * sr - ci * si) + flat[pl.ds(base + re_at, 8), :]
            im = e * (cr * si + ci * sr) + flat[pl.ds(base + im_at, 8), :]
            new.append((jnp.where(used, re, sr), jnp.where(used, im, si)))
        return tuple(new)

    zero = jnp.zeros((8, LANES), F32)
    state = lax.fori_loop(0, blocks, step, ((zero, zero),) * 4, unroll=4)
    for which, (kind, u_ref, o_ref) in enumerate(((WIDE, wu_ref, wo_ref), (NARROW, nu_ref, no_ref))):
        span = slice(which * 2 * LANES, (which + 1) * 2 * LANES)
        total = y_ref[:, span]
        for d in range(2):
            sr, si = state[d * 2 + which]
            for r in range(kind[0]):
                o_re, o_im = read_blocks(o_ref, d, r, kind)
                cr, ci = sr[r : r + 1], si[r : r + 1]
                row = jnp.concatenate([o_re * cr - o_im * ci, -(o_re * ci + o_im * cr)], axis=1)
                at = ((d * 12) + which * 8 + r) * 2 * LANES
                total += lax.dot_general(
                    decay_ref[:, at : at + 2 * LANES], group_block(row, r, kind), NT,
                    preferred_element_type=F32,
                )
        shaped = total + skip_ref[which : which + 1].astype(F32) * u_ref[...].astype(F32)
        inner = 0.7978845608028654 * (shaped + 0.044715 * (shaped * shaped * shaped))
        active = 0.5 * shaped * (1.0 + jnp.tanh(inner))
        hi = active.astype(BF16)
        lo = (active - hi.astype(F32)).astype(BF16)
        line = gate_ref[which].astype(F32)
        ids = lane_ids(line.shape) // 16
        gate = jnp.concatenate(
            [jnp.where(ids == g, line, 0.0).astype(BF16) for g in range(16)], axis=0
        )
        mixed = jnp.dot(hi, gate, preferred_element_type=F32) + jnp.dot(
            lo, gate, preferred_element_type=F32
        )
        out_ref[:, span] = (active * jax.nn.sigmoid(mixed)).astype(BF16)


SMEM = pl.BlockSpec(memory_space=pltpu.SMEM)
VMEM = pl.BlockSpec(memory_space=pltpu.VMEM)


def column(n):
    return pltpu.VMEM((8 * n, LANES), F32)


def mixer(me, wide_u, narrow_u, wide_p, narrow_p, steps, forget, wide_in, narrow_in, wide_out,
          narrow_out, skip, gate):
    blocks = lax.axis_size(SP)
    steps = steps.reshape(-1)
    forget = forget.reshape(-1, T)
    params = pltpu.CompilerParams(vmem_limit_bytes=32 * 2**20)
    shared = (wide_u, narrow_u, wide_p, narrow_p, wide_in, narrow_in, forget)
    send = pl.pallas_call(
        ends_kernel,
        out_shape=jax.ShapeDtypeStruct((blocks * 32, LANES), BF16),
        in_specs=[SMEM, SMEM] + [VMEM] * 7,
        out_specs=VMEM,
        scratch_shapes=[column(T)] * 12,
        compiler_params=params,
        name="ends",
    )(me, steps, *shared)
    got = lax.all_to_all(
        send.reshape(blocks, 32, LANES), SP, split_axis=0, concat_axis=0, tiled=True
    )
    y, decay = pl.pallas_call(
        local_kernel,
        out_shape=(
            jax.ShapeDtypeStruct((T, 4 * LANES), F32),
            jax.ShapeDtypeStruct((T, 24 * 2 * LANES), BF16),
        ),
        in_specs=[SMEM] + [VMEM] * 9 + [pl.BlockSpec(memory_space=pl.ANY)],
        out_specs=(VMEM, VMEM),
        scratch_shapes=[column(T)] * 20,
        compiler_params=params,
        name="local",
    )(steps, *shared, wide_out, narrow_out, send)
    return pl.pallas_call(
        carry_kernel,
        out_shape=jax.ShapeDtypeStruct((T, 4 * LANES), BF16),
        in_specs=[SMEM] + [VMEM] * 11,
        out_specs=VMEM,
        scratch_shapes=[pltpu.VMEM((blocks * 32, LANES), F32)] + [column(blocks)] * 4,
        compiler_params=params,
        name="carry",
    )(me, got.reshape(-1, LANES), wide_u, narrow_u, wide_p, narrow_p, wide_out, narrow_out, y,
      decay, skip, gate)


def ranks(routes):
    rows = routes.shape[0]
    earlier = jnp.arange(rows)[None, :] < jnp.arange(rows)[:, None]
    out = []
    for k in range(2):
        same = sum(
            (routes[:, k][:, None] == routes[:, o][None, :]).astype(jnp.int32) for o in range(2)
        )
        out.append(jnp.sum(jnp.where(earlier, same, 0), axis=1))
    return out


def local(
    wide_inputs, narrow_inputs, wide_poles, narrow_poles, step_sizes, forget, wide_in_map,
    narrow_in_map, wide_out_map, narrow_out_map, skip_weight, gate_mix, residual, mixer_gain,
    out_proj, ffn_gain, routes, route_weights, gate_proj, up_proj, down_proj,
):
    me = lax.axis_index(SP).astype(jnp.int32).reshape(1)
    gate_rows = jnp.transpose(gate_mix, (0, 2, 1, 3)).reshape(2, 16, 256)
    set_out = mixer(
        me, wide_inputs, narrow_inputs, wide_poles, narrow_poles, step_sizes, forget, wide_in_map,
        narrow_in_map, wide_out_map, narrow_out_map, skip_weight, gate_rows,
    )
    rows = residual.shape[0]
    width = residual.shape[1]
    both = lax.all_to_all(
        set_out.reshape(2, rows, 512), "tp", split_axis=0, concat_axis=0, tiled=True
    )
    joined = jnp.concatenate(
        [both[0, :, :256], both[1, :, :256], both[0, :, 256:], both[1, :, 256:]], axis=1
    ).astype(F32)
    scale = lax.rsqrt(jnp.mean(joined * joined, axis=1, keepdims=True) + EPS)
    mixed = (joined * scale * mixer_gain).astype(BF16)
    projected = jnp.dot(mixed, out_proj, preferred_element_type=F32)
    hidden1 = (residual.astype(F32) + projected).astype(BF16)
    hidden_wide = hidden1.astype(F32)
    normed = (
        hidden_wide
        * lax.rsqrt(jnp.mean(hidden_wide * hidden_wide, axis=1, keepdims=True) + EPS)
        * ffn_gain
    ).astype(BF16)
    experts = lax.axis_size(SP) * lax.axis_size("tp")
    place = [routes[:, k] * 2 + rank for k, rank in enumerate(ranks(routes))]
    slots = jnp.arange(2 * experts, dtype=jnp.int32)
    picks = [(slots[None, :] == at[:, None]).astype(BF16) for at in place]
    sections = lax.dot_general(
        picks[0] + picks[1], normed, (((0,), (0,)), ((), ())), preferred_element_type=F32
    ).astype(BF16)
    arrived = lax.all_to_all(
        sections.reshape(experts, 2, width), SP_TP, split_axis=0, concat_axis=0, tiled=True
    ).reshape(-1, width)
    gate_val = jnp.dot(arrived, gate_proj[0], preferred_element_type=F32)
    up_val = jnp.dot(arrived, up_proj[0], preferred_element_type=F32)
    expert_hidden = (jax.nn.silu(gate_val) * up_val).astype(BF16)
    done = jnp.dot(expert_hidden, down_proj[0], preferred_element_type=F32).astype(BF16)
    returned = lax.all_to_all(
        done.reshape(experts, 2, width), SP_TP, split_axis=0, concat_axis=0, tiled=True
    ).reshape(-1, width)
    share = route_weights / jnp.sum(route_weights, axis=1, keepdims=True)
    result = hidden_wide
    for k in range(2):
        taken = jnp.dot(picks[k], returned, preferred_element_type=F32)
        result = result + share[:, k : k + 1] * taken
    return result.astype(BF16)


def solution(mesh):
    finer = Mesh(mesh.devices.reshape(4, 4, 4, mesh.shape["tp"]), SP_TP)
    return jax.shard_map(
        local,
        mesh=finer,
        in_specs=(
            P(SP, "tp"),
            P(SP, "tp"),
            P(None, None, "tp", None),
            P(None, None, "tp", None),
            P(None, None, "tp"),
            P(None, None, "tp", SP),
            P(None, None, "tp", None, None),
            P(None, None, "tp", None, None),
            P(None, None, "tp", None, None),
            P(None, None, "tp", None, None),
            P(None, "tp"),
            P(None, "tp", None, None),
            P(SP_TP, None),
            P(),
            P(),
            P(),
            P(SP_TP, None),
            P(SP_TP, None),
            P(SP_TP, None, None),
            P(SP_TP, None, None),
            P(SP_TP, None, None),
        ),
        out_specs=P(SP_TP, None),
        check_vma=False,
    )
```

profile of v0, /device:TPU:1, one launch (start us, length us, event | category | flops | bytes accessed | tf_op | source)
XLA Modules:
  0.0 121.1 jit_solution(1273580704284885067)
XLA Ops:
  0.0 0.8 reshape.57.steps_ref
  0.8 1.0 copy-done
  1.8 1.0 copy-done.2
  2.9 0.8 copy-done.8
  3.7 0.8 copy-done.11
  4.5 0.8 copy-done.14
  5.3 0.8 copy-done.17
  6.1 0.8 copy-done.22
  6.8 0.0 copy-start.24
  6.9 4.7 %ends.1.after_ref = bf16[2048,128]{1,0:T(8,128)(2,1)} custom-call(s32[1]{0:T(128)} %bitcast.me_ref, f32[64]{0:T(128)S(1)} %reshape.57.steps_ref, bf16[128,256]{1,0:T(8,128)(2,1)S(1)} %copy-done.8, bf16[128,256]{1,0:T(8,128)(2,1)S(1)} %copy-done.11, f32[2,2,16,64]{3,2,1,0:T(8,128)S(1)} %copy-done.14, f32[2,2,16,32]{3,2,1,0:T(8,128)S(1)} %copy-done.17, ...), custom_call_target="tpu_custom_call" | custom-call | tf_op jit(solution)/shard_map/ends/pallas_call | solution.py:312
  11.5 12.1 %all-to-all-start = ((bf16[64,32,128]{2,1,0:T(8,128)(2,1)}), bf16[64,32,128]{2,1,0:T(8,128)(2,1)S(1)}, u32[]{:S(2)}, u32[]{:S(2)}) async-start(bf16[64,32,128]{2,1,0:T(8,128)(2,1)} %bitcast.2), calls=%async_computation | async-start | bytes 1048576 | tf_op jit(solution)/shard_map/all_to_all | solution.py:321
  23.6 0.9 copy.23
  24.5 0.2 reshape.61.gate_ref
  24.7 0.0 copy-start.1
  24.7 1.0 copy-done.1
  25.8 1.0 copy-done.3
  26.8 1.0 copy-done.4
  27.8 1.0 copy-done.6
  28.9 0.8 copy-done.9
  29.7 0.8 copy-done.12
  30.6 0.8 copy-done.15
  31.3 0.8 copy-done.18
  32.1 0.8 copy-done.23
  32.8 5.5 %local.1 = (f32[128,512]{1,0:T(8,128)S(1)}, bf16[128,6144]{1,0:T(8,128)(2,1)S(1)}) custom-call(f32[64]{0:T(128)S(1)} %reshape.57.steps_ref, bf16[128,256]{1,0:T(8,128)(2,1)S(1)} %copy-done.9, bf16[128,256]{1,0:T(8,128)(2,1)S(1)} %copy-done.12, f32[2,2,16,64]{3,2,1,0:T(8,128)S(1)} %copy-done.15, f32[2,2,16,32]{3,2,1,0:T(8,128)S(1)} %copy-done.18, ...), custom_call_target="tpu_custom_call" | custom-call | tf_op jit(solution)/shard_map/local/pallas_call | solution.py:324
  38.4 0.0 copy-start.20
  38.4 0.7 copy-done.20
  39.1 0.2 select_reduce_fusion.1
  39.3 0.0 all-to-all-done
  39.4 0.0 copy-start.21
  39.4 0.9 copy-done.21
  40.3 3.3 %carry.1 = bf16[128,512]{1,0:T(8,128)(2,1)S(1)} custom-call(s32[1]{0:T(128)} %bitcast.me_ref, bf16[2048,128]{1,0:T(8,128)(2,1)S(1)} %bitcast.58, bf16[128,256]{1,0:T(8,128)(2,1)S(1)} %copy-done.10, bf16[128,256]{1,0:T(8,128)(2,1)S(1)} %copy-done.13, f32[2,2,16,64]{3,2,1,0:T(8,128)S(1)} %copy-done.16, f32[2,2,16,32]{3,2,1,0:T(8,128)S(1)} %copy-done.19, ...), custom_call_target="tpu_custom_call" | custom-call | tf_op jit(solution)/shard_map/carry/pallas_call | solution.py:336
  43.6 4.4 %all_to_all.20 = bf16[2,64,512]{2,1,0:T(8,128)(2,1)S(1)} all-to-all(bf16[2,64,512]{2,1,0:T(8,128)(2,1)S(1)} %bitcast.59), channel_id=1, replica_groups=mesh['sp_0'=4,'sp_1'=4,'sp_2'=4,'tp'=2] {'tp'}, dimensions={0} | all-to-all | bytes 262144 | tf_op jit(solution)/shard_map/all_to_all | solution.py:373
  48.0 0.1 fusion.23
  48.2 2.0 %multiply_reduce_fusion = (f32[64]{0:T(128)S(1)}, f32[64,2048]{1,0:T(8,128)S(1)}) fusion(bf16[1024,2048]{1,0:T(8,128)(2,1)S(1)} %copy-done.25, f32[1024]{0:T(1024)S(1)} %copy-done.27, f32[64]{0:T(128)S(1)} %add_rsqrt_fusion.1, bf16[64,256]{1,0:T(8,128)(2,1)S(1)} %get-tuple-element.12, bf16[64,256]{1,0:T(8,128)(2,1)S(1)} %get-tuple-element.13, ...), kind=kOutput, calls=%fused_computation.20 | convolution fusion | flops 269942720 | bytes 5116416 | tf_op jit(solution)/shard_map/dot_general | solution.py:381
  50.2 0.0 copy-done.26
  50.2 0.5 convolution_convert_fusion
  50.8 0.7 reshape.63
  51.5 28.3 %all_to_all.21 = bf16[128,2,2048]{2,1,0:T(2,128)(2,1)S(1)} all-to-all(bf16[128,2,2048]{2,1,0:T(2,128)(2,1)S(1)} %reshape.63), channel_id=1, replica_groups=mesh['sp_0'=4,'sp_1'=4,'sp_2'=4,'tp'=2] {'sp_0','sp_1','sp_2','tp'}, dimensions={0} | all-to-all | bytes 2097152 | tf_op jit(solution)/shard_map/all_to_all | solution.py:396
  79.8 0.4 reshape.64
  80.2 5.6 %fusion.4 = f32[256,1408]{1,0:T(8,128)} fusion(bf16[256,2048]{1,0:T(8,128)(2,1)S(1)} %reshape.64, bf16[1,2048,1408]{2,1,0:T(8,128)(2,1)} %param.39), kind=kOutput, calls=%fused_computation.4 | convolution fusion | flops 1476395008 | bytes 8257536 | tf_op jit(solution)/shard_map/dot_general | solution.py:399
  85.8 8.2 %fusion.12 = bf16[256,2048]{1,0:T(8,128)(2,1)S(1)} fusion(bf16[1,1408,2048]{2,1,0:T(8,128)(2,1)} %param.41, bf16[256,2048]{1,0:T(8,128)(2,1)S(1)} %reshape.64, bf16[1,2048,1408]{2,1,0:T(8,128)(2,1)} %param.40, f32[256,1408]{1,0:T(8,128)} %fusion.4), kind=kOutput, calls=%fused_computation.8 | convolution fusion | flops 2955476992 | bytes 15073280 | tf_op jit(solution)/shard_map/dot_general | solution.py:402
  94.0 0.0 copy-start.29
  94.0 1.5 %reshape.65 = bf16[128,2,2048]{2,1,0:T(2,128)(2,1)} reshape(bf16[256,2048]{1,0:T(8,128)(2,1)S(1)} %fusion.12) | data formatting | bytes 2097152 | tf_op jit(solution)/shard_map/reshape | solution.py:404
  95.5 4.4 %all-to-all-start.3 = ((bf16[128,2,2048]{2,1,0:T(2,128)(2,1)}), bf16[128,2,2048]{2,1,0:T(2,128)(2,1)S(1)}, u32[]{:S(2)}, u32[]{:S(2)}) async-start(bf16[128,2,2048]{2,1,0:T(2,128)(2,1)} %reshape.65), calls=%async_computation.3 | async-start | bytes 2097152 | tf_op jit(solution)/shard_map/all_to_all | solution.py:403
  100.0 19.3 %all-to-all-done.3 = bf16[128,2,2048]{2,1,0:T(2,128)(2,1)S(1)} async-done(((bf16[128,2,2048]{2,1,0:T(2,128)(2,1)}), bf16[128,2,2048]{2,1,0:T(2,128)(2,1)S(1)}, u32[]{:S(2)}, u32[]{:S(2)}) %all-to-all-start.3) | async-done | bytes 1048608 | tf_op jit(solution)/shard_map/all_to_all | solution.py:403
  119.3 0.4 reshape.66
  119.7 0.3 fusion.16
  120.0 1.0 fusion.19
  (44 shorter events, 0.1 us)
Async XLA Ops:
  0.0 39.3 %copy-start.16 = (f32[2,2,16,64]{3,2,1,0:T(8,128)S(1)}, f32[2,2,16,64]{3,2,1,0:T(8,128)}, u32[]{:S(2)}) copy-start(f32[2,2,16,64]{3,2,1,0:T(8,128)} %wp_ref.5) | copy-start | bytes 49156
  0.8 1.0 copy-start
  1.8 1.0 copy-start.2
  2.9 0.8 copy-start.8
  3.7 0.8 copy-start.11
  4.5 0.8 copy-start.14
  5.3 0.8 copy-start.17
  6.1 0.8 copy-start.22
  6.8 32.3 %copy-start.28 = (s32[64,2]{0,1:T(2,128)S(1)}, s32[64,2]{0,1:T(2,128)}, u32[]{:S(2)}) copy-start(s32[64,2]{0,1:T(2,128)} %param.37) | copy-start | bytes 1540
  6.8 32.5 %copy-start.5 = (f32[2,2,16,16,64]{4,3,2,1,0:T(8,128)S(1)}, f32[2,2,16,16,64]{4,3,2,1,0:T(8,128)}, u32[]{:S(2)}) copy-start(f32[2,2,16,16,64]{4,3,2,1,0:T(8,128)} %wo_ref.3) | copy-start | bytes 786436
  6.8 32.5 %copy-start.7 = (f32[2,2,16,16,32]{4,3,2,1,0:T(8,128)S(1)}, f32[2,2,16,16,32]{4,3,2,1,0:T(8,128)}, u32[]{:S(2)}) copy-start(f32[2,2,16,16,32]{4,3,2,1,0:T(8,128)} %no_ref.3) | copy-start | bytes 393220
  6.8 32.5 %copy-start.10 = (bf16[128,256]{1,0:T(8,128)(2,1)S(1)}, bf16[128,256]{1,0:T(8,128)(2,1)}, u32[]{:S(2)}) copy-start(bf16[128,256]{1,0:T(8,128)(2,1)} %wu_ref.5) | copy-start | bytes 196612
  6.8 32.5 %copy-start.13 = (bf16[128,256]{1,0:T(8,128)(2,1)S(1)}, bf16[128,256]{1,0:T(8,128)(2,1)}, u32[]{:S(2)}) copy-start(bf16[128,256]{1,0:T(8,128)(2,1)} %nu_ref.5) | copy-start | bytes 196612
  6.8 32.5 %copy-start.19 = (f32[2,2,16,32]{3,2,1,0:T(8,128)S(1)}, f32[2,2,16,32]{3,2,1,0:T(8,128)}, u32[]{:S(2)}) copy-start(f32[2,2,16,32]{3,2,1,0:T(8,128)} %np_ref.5) | copy-start | bytes 24580
  6.8 32.5 %copy-start.24 = (bf16[2,256]{1,0:T(2,128)(2,1)S(1)}, bf16[2,256]{1,0:T(2,128)(2,1)}, u32[]{:S(2)}) copy-start(bf16[2,256]{1,0:T(2,128)(2,1)} %skip_ref.1) | copy-start | bytes 3076
  11.5 36.7 %copy-start.27 = (f32[1024]{0:T(1024)S(1)}, f32[1024]{0:T(1024)}, u32[]{:S(2)}) copy-start(f32[1024]{0:T(1024)} %param.34) | copy-start | bytes 12292
  11.5 27.8 %all-to-all-start = ((bf16[64,32,128]{2,1,0:T(8,128)(2,1)}), bf16[64,32,128]{2,1,0:T(8,128)(2,1)S(1)}, u32[]{:S(2)}, u32[]{:S(2)}) async-start(bf16[64,32,128]{2,1,0:T(8,128)(2,1)} %bitcast.2), calls=%async_computation | async-start | bytes 1048576 | tf_op jit(solution)/shard_map/all_to_all | solution.py:321
  24.7 1.0 copy-start.1
  25.8 1.0 copy-start.3
  26.8 1.0 copy-start.4
  27.8 1.0 copy-start.6
  28.9 0.8 copy-start.9
  29.7 0.8 copy-start.12
  30.6 0.8 copy-start.15
  31.3 0.8 copy-start.18
  32.1 0.8 copy-start.23
  38.4 0.7 copy-start.20
  39.4 1.0 copy-start.21
  40.3 7.9 %copy-start.25 = (bf16[1024,2048]{1,0:T(8,128)(2,1)S(1)}, bf16[1024,2048]{1,0:T(8,128)(2,1)}, u32[]{:S(2)}) copy-start(bf16[1024,2048]{1,0:T(8,128)(2,1)} %param.35) | copy-start | bytes 12582916
  40.3 9.9 %copy-start.26 = (f32[2048]{0:T(1024)S(1)}, f32[2048]{0:T(1024)}, u32[]{:S(2)}) copy-start(f32[2048]{0:T(1024)} %param.36) | copy-start | bytes 24580
  94.0 6.0 %copy-start.29 = (f32[64,2]{0,1:T(2,128)S(1)}, f32[64,2]{0,1:T(2,128)}, u32[]{:S(2)}) copy-start(f32[64,2]{0,1:T(2,128)} %param.38) | copy-start | bytes 1540
  95.5 23.8 %all-to-all-start.3 = ((bf16[128,2,2048]{2,1,0:T(2,128)(2,1)}), bf16[128,2,2048]{2,1,0:T(2,128)(2,1)S(1)}, u32[]{:S(2)}, u32[]{:S(2)}) async-start(bf16[128,2,2048]{2,1,0:T(2,128)(2,1)} %reshape.65), calls=%async_computation.3 | async-start | bytes 2097152 | tf_op jit(solution)/shard_map/all_to_all | solution.py:403
where the time goes:
time: 122 us; the launch traced here: 121 us
  blocking collectives  32.7 us (27%)
  local copies, waits for them, and re-layouts  20.8 us (17%)
  waiting for transfers between devices  19.3 us (16%)
  matrix products  17.7 us (15%)
  starting transfers between devices  16.5 us (14%)
  Pallas kernels  13.4 us (11%)
    all_to_all x1, blocking collectives, local(): lax.all_to_all(sections.reshape(experts, 2, width), SP_TP, split_axis=0,...  28.3 us
    all_to_all x1, waiting for transfers between devices, local(): lax.all_to_all(done.reshape(experts, 2, width), SP_TP, split_axis=0, conc...  19.3 us
    unnamed x60, local copies, waits for them, and re-layouts  15.8 us
    all_to_all x1, starting transfers between devices, mixer(): lax.all_to_all(send.reshape(blocks, 32, LANES), SP, split_axis=0, concat_...  12.1 us
    dot_general x1, matrix products, local(): jnp.dot(expert_hidden, down_proj[0], preferred_element_type=F32)  8.19 us
    dot_general x1, matrix products, local(): gate_val = jnp.dot(arrived, gate_proj[0], preferred_element_type=F32)  5.56 us
    pallas_call x1, Pallas kernels, mixer(): pl.pallas_call(local_kernel, out_shape=(jax.ShapeDtypeStruct((T, 4 * LANE...  5.53 us
    pallas_call x1, Pallas kernels, mixer(): pl.pallas_call(ends_kernel, out_shape=jax.ShapeDtypeStruct((blocks * 32,...  4.65 us
  transfers between devices with their start and end apart: 2, of which 1 were waited for; matrix products, arithmetic and copies ran while one was open for 1% of the time, Pallas kernels for 5%

commit v1 on v0

--- a/solution.py
+++ b/solution.py
@@ -18,6 +18,21 @@
 NT = (((1,), (1,)), ((), ()))
 WIDE = (8, 2, 64)
 NARROW = (4, 4, 32)
+
+
+def started(sources, buffers, sems):
+    copies = [
+        pltpu.make_async_copy(source, buffer, sems.at[k])
+        for k, (source, buffer) in enumerate(zip(sources, buffers))
+    ]
+    for copy in copies:
+        copy.start()
+    return copies
+
+
+def fetch(sources, buffers, sems):
+    for copy in started(sources, buffers, sems):
+        copy.wait()
 
 
 def lane_ids(shape):
@@ -125,9 +140,10 @@
     return hi, mid, x - hi - mid
 
 
-def ends_kernel(
-    me_ref, steps_ref, wu_ref, nu_ref, wp_ref, np_ref, wi_ref, ni_ref, forget_ref, send_ref, *scr
-):
+def ends_kernel(me_ref, steps_ref, *refs):
+    sources, send_ref, buffers, sems, scr = refs[:7], refs[7], refs[8:15], refs[15], refs[16:]
+    fetch(sources, buffers, sems)
+    wu_ref, nu_ref, wp_ref, np_ref, wi_ref, ni_ref, forget_ref = buffers
     forget_t = forget_columns(forget_ref)
     turns = load_pushes(
         steps_ref, (wu_ref, nu_ref), (wp_ref, np_ref), (wi_ref, ni_ref), forget_t, scr
@@ -175,11 +191,11 @@
     return side_by_side(out_ref[d, 0], r, kind), side_by_side(out_ref[d, 1], r, kind)
 
 
-def local_kernel(
-    steps_ref, wu_ref, nu_ref, wp_ref, np_ref, wi_ref, ni_ref, forget_ref, wo_ref, no_ref, after_ref,
-    y_ref, decay_ref, *scr
-):
-    del after_ref
+def local_kernel(steps_ref, *refs):
+    sources, results, buffers = refs[:9], refs[10:12], refs[12:21]
+    sems, y_ref, decay_ref, out_sems, scr = refs[21], refs[22], refs[23], refs[24], refs[25:]
+    fetch(sources, buffers, sems)
+    wu_ref, nu_ref, wp_ref, np_ref, wi_ref, ni_ref, forget_ref, wo_ref, no_ref = buffers
     turns = load_pushes(
         steps_ref, (wu_ref, nu_ref), (wp_ref, np_ref), (wi_ref, ni_ref),
         forget_columns(forget_ref), scr,
@@ -222,12 +238,16 @@
                 first = ((d * 12) + which * 8 + r) * 2 * LANES
                 decay_ref[:, first : first + 2 * LANES] = decay.astype(BF16)
         y_ref[:, which * 2 * LANES : (which + 1) * 2 * LANES] = total
-
-
-def carry_kernel(
-    me_ref, got_ref, wu_ref, nu_ref, wp_ref, np_ref, wo_ref, no_ref, y_ref, decay_ref, skip_ref,
-    gate_ref, out_ref, flat, *kept
-):
+    fetch((y_ref, decay_ref), results, out_sems)
+
+
+def carry_kernel(me_ref, got_ref, *refs):
+    sources, out_ref, weights_ref, buffers = refs[:11], refs[11], refs[12], refs[13:23]
+    sems, flat, kept = refs[23], refs[24], refs[25:]
+    copies = started(sources, buffers + (weights_ref,), sems)
+    wp_ref, np_ref, wu_ref, nu_ref, wo_ref, no_ref, skip_ref, gate_ref, y_ref, decay_ref = buffers
+    for copy in copies[:2]:
+        copy.wait()
     me = me_ref[0]
     blocks = got_ref.shape[0] // 32
     flat[...] = got_ref[...].astype(F32)
@@ -264,6 +284,8 @@
 
     zero = jnp.zeros((8, LANES), F32)
     state = lax.fori_loop(0, blocks, step, ((zero, zero),) * 4, unroll=4)
+    for copy in copies[2:10]:
+        copy.wait()
     for which, (kind, u_ref, o_ref) in enumerate(((WIDE, wu_ref, wo_ref), (NARROW, nu_ref, no_ref))):
         span = slice(which * 2 * LANES, (which + 1) * 2 * LANES)
         total = y_ref[:, span]
@@ -292,57 +314,174 @@
             lo, gate, preferred_element_type=F32
         )
         out_ref[:, span] = (active * jax.nn.sigmoid(mixed)).astype(BF16)
+    copies[10].wait()
 
 
 SMEM = pl.BlockSpec(memory_space=pltpu.SMEM)
 VMEM = pl.BlockSpec(memory_space=pltpu.VMEM)
+HBM = pl.BlockSpec(memory_space=pltpu.HBM)
+MIB = 2**20
 
 
 def column(n):
     return pltpu.VMEM((8 * n, LANES), F32)
 
 
+def fetched(arrays):
+    return [pltpu.VMEM(a.shape, a.dtype) for a in arrays] + [
+        pltpu.SemaphoreType.DMA((len(arrays),))
+    ]
+
+
+def far(arrays):
+    return tuple(pltpu.with_memory_space_constraint(a, pltpu.HBM) for a in arrays)
+
+
+def grant(mib):
+    return pltpu.CompilerParams(vmem_limit_bytes=mib * MIB)
+
+
 def mixer(me, wide_u, narrow_u, wide_p, narrow_p, steps, forget, wide_in, narrow_in, wide_out,
-          narrow_out, skip, gate):
+          narrow_out, skip, gate, out_proj):
     blocks = lax.axis_size(SP)
     steps = steps.reshape(-1)
     forget = forget.reshape(-1, T)
-    params = pltpu.CompilerParams(vmem_limit_bytes=32 * 2**20)
-    shared = (wide_u, narrow_u, wide_p, narrow_p, wide_in, narrow_in, forget)
+    shared = far((wide_u, narrow_u, wide_p, narrow_p, wide_in, narrow_in, forget))
     send = pl.pallas_call(
         ends_kernel,
         out_shape=jax.ShapeDtypeStruct((blocks * 32, LANES), BF16),
-        in_specs=[SMEM, SMEM] + [VMEM] * 7,
+        in_specs=[SMEM, SMEM] + [HBM] * 7,
         out_specs=VMEM,
-        scratch_shapes=[column(T)] * 12,
-        compiler_params=params,
+        scratch_shapes=fetched(shared) + [column(T)] * 12,
+        compiler_params=grant(20),
         name="ends",
     )(me, steps, *shared)
     got = lax.all_to_all(
         send.reshape(blocks, 32, LANES), SP, split_axis=0, concat_axis=0, tiled=True
     )
+    sources = shared + far((wide_out, narrow_out))
     y, decay = pl.pallas_call(
         local_kernel,
         out_shape=(
-            jax.ShapeDtypeStruct((T, 4 * LANES), F32),
-            jax.ShapeDtypeStruct((T, 24 * 2 * LANES), BF16),
+            pltpu.HBM((T, 4 * LANES), F32),
+            pltpu.HBM((T, 24 * 2 * LANES), BF16),
         ),
-        in_specs=[SMEM] + [VMEM] * 9 + [pl.BlockSpec(memory_space=pl.ANY)],
-        out_specs=(VMEM, VMEM),
-        scratch_shapes=[column(T)] * 20,
-        compiler_params=params,
+        in_specs=[SMEM] + [HBM] * 10,
+        out_specs=(HBM, HBM),
+        scratch_shapes=fetched(sources)
+        + [pltpu.VMEM((T, 4 * LANES), F32), pltpu.VMEM((T, 24 * 2 * LANES), BF16)]
+        + [pltpu.SemaphoreType.DMA((2,))] + [column(T)] * 20,
+        compiler_params=grant(24),
         name="local",
-    )(steps, *shared, wide_out, narrow_out, send)
+    )(steps, *sources, send)
+    sources = far(
+        (wide_p, narrow_p, wide_u, narrow_u, wide_out, narrow_out, skip, gate, y, decay, out_proj)
+    )
     return pl.pallas_call(
         carry_kernel,
-        out_shape=jax.ShapeDtypeStruct((T, 4 * LANES), BF16),
-        in_specs=[SMEM] + [VMEM] * 11,
-        out_specs=VMEM,
-        scratch_shapes=[pltpu.VMEM((blocks * 32, LANES), F32)] + [column(blocks)] * 4,
-        compiler_params=params,
+        out_shape=(
+            jax.ShapeDtypeStruct((T, 4 * LANES), BF16),
+            jax.ShapeDtypeStruct(out_proj.shape, BF16),
+        ),
+        in_specs=[SMEM, VMEM] + [HBM] * 11,
+        out_specs=(VMEM, VMEM),
+        scratch_shapes=[pltpu.VMEM(a.shape, a.dtype) for a in sources[:10]]
+        + [pltpu.SemaphoreType.DMA((11,))]
+        + [pltpu.VMEM((blocks * 32, LANES), F32)] + [column(blocks)] * 4,
+        compiler_params=grant(20),
         name="carry",
-    )(me, got.reshape(-1, LANES), wide_u, narrow_u, wide_p, narrow_p, wide_out, narrow_out, y,
-      decay, skip, gate)
+    )(me, got.reshape(-1, LANES), *sources)
+
+
+def project_kernel(
+    core_ref, mine_ref, other_ref, rows_ref, gain_ref, ffn_ref, residual_ref, proj_ref, hidden_ref,
+    send_ref,
+):
+    swap = core_ref[0] == 1
+    mine, other = mine_ref[...].astype(F32), other_ref[...].astype(F32)
+    first, second = jnp.where(swap, other, mine), jnp.where(swap, mine, other)
+    half = first.shape[1] // 2
+    joined = jnp.concatenate(
+        [first[:, :half], second[:, :half], first[:, half:], second[:, half:]], axis=1
+    )
+    scale = lax.rsqrt(jnp.mean(joined * joined, axis=1, keepdims=True) + EPS)
+    mixed = (joined * scale * gain_ref[...]).astype(BF16)
+    projected = jnp.dot(mixed, proj_ref[...], preferred_element_type=F32)
+    hidden1 = (residual_ref[...].astype(F32) + projected).astype(BF16)
+    hidden_ref[...] = hidden1
+    wide = hidden1.astype(F32)
+    scale = lax.rsqrt(jnp.mean(wide * wide, axis=1, keepdims=True) + EPS)
+    normed = (wide * scale * ffn_ref[...]).astype(BF16)
+    quarter = normed.shape[1] // 4
+    stacked = jnp.concatenate([normed[:, q * quarter : (q + 1) * quarter] for q in range(4)], axis=0)
+    size = stacked.shape[0]
+    for b in range(send_ref.shape[0] // size):
+        ids = lax.broadcasted_iota(jnp.int32, (size, size), 0) + b * size
+        hit = (ids == rows_ref[0:1, :]) | (ids == rows_ref[1:2, :])
+        pick = jnp.where(hit, 1.0, 0.0).astype(BF16)
+        send_ref[b * size : (b + 1) * size, :] = jnp.dot(
+            pick, stacked, preferred_element_type=F32
+        ).astype(BF16)
+
+
+def turned(back):
+    out = lax.broadcasted_iota(jnp.int32, (256, 256), 0)
+    src = lax.broadcasted_iota(jnp.int32, (256, 256), 1)
+    if back:
+        out, src = src, out
+    wanted = ((out % 64) // 2) * 8 + (out // 64) * 2 + out % 2
+    return jnp.where(src == wanted, 1.0, 0.0).astype(BF16)
+
+
+def experts_kernel(
+    in_ref, gate_ref, up_ref, far_ref, out_ref, x_ref, h_ref, down_ref, sem
+):
+    copy = pltpu.make_async_copy(far_ref, down_ref, sem)
+    copy.start()
+    quarter = in_ref.shape[1]
+    turn = turned(False)
+    for b in range(4):
+        got = jnp.dot(
+            turn, in_ref[b * 256 : (b + 1) * 256, :], preferred_element_type=F32
+        ).astype(BF16)
+        for q in range(4):
+            x_ref[b * 64 : (b + 1) * 64, q * quarter : (q + 1) * quarter] = got[
+                q * 64 : (q + 1) * 64
+            ]
+    x = x_ref[...]
+    gate = jnp.dot(x, gate_ref[...], preferred_element_type=F32)
+    up = jnp.dot(x, up_ref[...], preferred_element_type=F32)
+    h_ref[...] = (gate * jax.nn.sigmoid(gate) * up).astype(BF16)
+    copy.wait()
+    done = jnp.dot(h_ref[...], down_ref[...], preferred_element_type=F32).astype(BF16)
+    back = turned(True)
+    for b in range(4):
+        stacked = jnp.concatenate(
+            [
+                done[b * 64 : (b + 1) * 64, q * quarter : (q + 1) * quarter] for q in range(4)
+            ],
+            axis=0,
+        )
+        out_ref[b * 256 : (b + 1) * 256, :] = jnp.dot(
+            back, stacked, preferred_element_type=F32
+        ).astype(BF16)
+
+
+def combine_kernel(got_ref, cols_ref, weights_ref, hidden_ref, out_ref):
+    w = weights_ref[...]
+    total = w[:, 0:1] + w[:, 1:2]
+    rows = hidden_ref.shape[0]
+    quarter = got_ref.shape[1]
+    size = got_ref.shape[0]
+    got = got_ref[...]
+    result = hidden_ref[...].astype(F32)
+    ids = lax.broadcasted_iota(jnp.int32, (4 * rows, size), 1)
+    for k in range(2):
+        pick = jnp.where(ids == cols_ref[:, k : k + 1], 1.0, 0.0).astype(BF16)
+        taken = jnp.dot(pick, got, preferred_element_type=F32)
+        taken = jnp.concatenate([taken[q * rows : (q + 1) * rows] for q in range(4)], axis=1)
+        result = result + (w[:, k : k + 1] / total) * taken
+    out_ref[...] = result.astype(BF16)
 
 
 def ranks(routes):
@@ -364,51 +503,61 @@
 ):
     me = lax.axis_index(SP).astype(jnp.int32).reshape(1)
     gate_rows = jnp.transpose(gate_mix, (0, 2, 1, 3)).reshape(2, 16, 256)
-    set_out = mixer(
+    set_out, near_proj = mixer(
         me, wide_inputs, narrow_inputs, wide_poles, narrow_poles, step_sizes, forget, wide_in_map,
-        narrow_in_map, wide_out_map, narrow_out_map, skip_weight, gate_rows,
+        narrow_in_map, wide_out_map, narrow_out_map, skip_weight, gate_rows, out_proj,
     )
     rows = residual.shape[0]
     width = residual.shape[1]
-    both = lax.all_to_all(
-        set_out.reshape(2, rows, 512), "tp", split_axis=0, concat_axis=0, tiled=True
-    )
-    joined = jnp.concatenate(
-        [both[0, :, :256], both[1, :, :256], both[0, :, 256:], both[1, :, 256:]], axis=1
-    ).astype(F32)
-    scale = lax.rsqrt(jnp.mean(joined * joined, axis=1, keepdims=True) + EPS)
-    mixed = (joined * scale * mixer_gain).astype(BF16)
-    projected = jnp.dot(mixed, out_proj, preferred_element_type=F32)
-    hidden1 = (residual.astype(F32) + projected).astype(BF16)
-    hidden_wide = hidden1.astype(F32)
-    normed = (
-        hidden_wide
-        * lax.rsqrt(jnp.mean(hidden_wide * hidden_wide, axis=1, keepdims=True) + EPS)
-        * ffn_gain
-    ).astype(BF16)
+    core = lax.axis_index("tp").astype(jnp.int32)
+    halves = set_out.reshape(2, rows, 512)
+    mine = lax.dynamic_index_in_dim(halves, core, 0, keepdims=False)
+    other = lax.dynamic_index_in_dim(halves, 1 - core, 0, keepdims=False)
+    other = lax.ppermute(other, "tp", [(0, 1), (1, 0)])
     experts = lax.axis_size(SP) * lax.axis_size("tp")
-    place = [routes[:, k] * 2 + rank for k, rank in enumerate(ranks(routes))]
-    slots = jnp.arange(2 * experts, dtype=jnp.int32)
-    picks = [(slots[None, :] == at[:, None]).astype(BF16) for at in place]
-    sections = lax.dot_general(
-        picks[0] + picks[1], normed, (((0,), (0,)), ((), ())), preferred_element_type=F32
-    ).astype(BF16)
-    arrived = lax.all_to_all(
-        sections.reshape(experts, 2, width), SP_TP, split_axis=0, concat_axis=0, tiled=True
-    ).reshape(-1, width)
-    gate_val = jnp.dot(arrived, gate_proj[0], preferred_element_type=F32)
-    up_val = jnp.dot(arrived, up_proj[0], preferred_element_type=F32)
-    expert_hidden = (jax.nn.silu(gate_val) * up_val).astype(BF16)
-    done = jnp.dot(expert_hidden, down_proj[0], preferred_element_type=F32).astype(BF16)
-    returned = lax.all_to_all(
-        done.reshape(experts, 2, width), SP_TP, split_axis=0, concat_axis=0, tiled=True
-    ).reshape(-1, width)
-    share = route_weights / jnp.sum(route_weights, axis=1, keepdims=True)
-    result = hidden_wide
-    for k in range(2):
-        taken = jnp.dot(picks[k], returned, preferred_element_type=F32)
-        result = result + share[:, k : k + 1] * taken
-    return result.astype(BF16)
+    quarters = jnp.repeat(jnp.arange(4, dtype=jnp.int32) * 2, rows)
+    places = jnp.stack(
+        [jnp.tile(routes[:, k] * 8 + rank, 4) + quarters for k, rank in enumerate(ranks(routes))]
+    )
+    hidden1, send = pl.pallas_call(
+        project_kernel,
+        out_shape=(
+            jax.ShapeDtypeStruct((rows, width), BF16),
+            jax.ShapeDtypeStruct((experts * 8, width // 4), BF16),
+        ),
+        in_specs=[SMEM] + [VMEM] * 7,
+        out_specs=(VMEM, VMEM),
+        compiler_params=grant(12),
+        name="project",
+    )(
+        core.reshape(1), mine, other, places, mixer_gain.reshape(1, -1), ffn_gain.reshape(1, -1),
+        residual, near_proj,
+    )
+    exchange = lambda x: lax.all_to_all(
+        x.reshape(experts, 8, width // 4), SP_TP, split_axis=0, concat_axis=0, tiled=True
+    ).reshape(-1, width // 4)
+    done = pl.pallas_call(
+        experts_kernel,
+        out_shape=jax.ShapeDtypeStruct((experts * 8, width // 4), BF16),
+        in_specs=[VMEM] * 3 + [HBM],
+        out_specs=VMEM,
+        scratch_shapes=[
+            pltpu.VMEM((2 * experts, width), BF16),
+            pltpu.VMEM((2 * experts, gate_proj.shape[2]), BF16),
+            pltpu.VMEM(down_proj.shape[1:], BF16),
+            pltpu.SemaphoreType.DMA,
+        ],
+        compiler_params=grant(20),
+        name="experts",
+    )(exchange(send), gate_proj[0], up_proj[0], *far((down_proj[0],)))
+    return pl.pallas_call(
+        combine_kernel,
+        out_shape=jax.ShapeDtypeStruct((rows, width), BF16),
+        in_specs=[VMEM] * 4,
+        out_specs=VMEM,
+        compiler_params=grant(12),
+        name="combine",
+    )(exchange(done), places.T, route_weights, hidden1)
 
 
 def solution(mesh):

time: 122 us -> 102 us (0.84)
  matrix products: 17.7 us -> 0 us
  Pallas kernels: 13.4 us -> 31 us
  local copies, waits for them, and re-layouts: 20.8 us -> 3.71 us
  blocking collectives: 32.7 us -> 27.1 us
  starting transfers between devices: 16.5 us -> 18.6 us
    dot_general x6 -> x0, matrix products: 17.7 us -> none  [the longest x1 8.19 us: local(): jnp.dot(expert_hidden, down_proj[0], preferred_element_type=F32)]
    pallas_call x2 -> x5, Pallas kernels: 8.8 us -> 25 us  [the longest x1 9.24 us: local(): pl.pallas_call(experts_kernel, out_shape=jax.ShapeDtypeStruct((experts *...]
    unnamed x60 -> x17, local copies, waits for them, and re-layouts: 15.8 us -> 0.14 us
    all_to_all x2 -> x1, blocking collectives: 32.7 us -> 27.1 us  [local(): lax.all_to_all(x.reshape(experts, 8, width // 4), SP_TP, split_axis=0, co...]
    reshape x4 -> x0, local copies, waits for them, and re-layouts: 3.06 us -> none  [the longest x1 1.51 us: local(): done.reshape(experts, 2, width)]
    ppermute x0 -> x1, starting transfers between devices: none -> 2.21 us  [local(): other = lax.ppermute(other, 'tp', [(0, 1), (1, 0)])]
    pallas_call x1, Pallas kernels: 4.65 us -> 6 us  [mixer(): pl.pallas_call(ends_kernel, out_shape=jax.ShapeDtypeStruct((blocks * 32,...]
  transfers between devices with their start and end apart: 2 -> 3, of which waited for: 1 -> 2; matrix products, arithmetic and copies ran while one was open for 1% -> 4% of each run, Pallas kernels for 5% -> 8%
where the time goes in v1:
time: 102 us
  Pallas kernels  31 us (30%)
  blocking collectives  27.1 us (27%)
  waiting for transfers between devices  20 us (20%)
  starting transfers between devices  18.6 us (18%)
  local copies, waits for them, and re-layouts  3.71 us (4%)
  other arithmetic  1.03 us (1%)
    all_to_all x1, blocking collectives, local(): lax.all_to_all(x.reshape(experts, 8, width // 4), SP_TP, split_axis=0, co...  27.1 us
    all_to_all x1, waiting for transfers between devices, local(): lax.all_to_all(x.reshape(experts, 8, width // 4), SP_TP, split_axis=0, co...  19.1 us
    all_to_all x1, starting transfers between devices, mixer(): lax.all_to_all(send.reshape(blocks, 32, LANES), SP, split_axis=0, concat_...  12 us
    pallas_call x1, Pallas kernels, local(): pl.pallas_call(experts_kernel, out_shape=jax.ShapeDtypeStruct((experts *...  9.24 us
    pallas_call x1, Pallas kernels, mixer(): pl.pallas_call(local_kernel, out_shape=(pltpu.HBM((T, 4 * LANES), F32), p...  8.4 us
    pallas_call x1, Pallas kernels, mixer(): pl.pallas_call(ends_kernel, out_shape=jax.ShapeDtypeStruct((blocks * 32,...  6 us
    all_to_all x1, starting transfers between devices, local(): lax.all_to_all(x.reshape(experts, 8, width // 4), SP_TP, split_axis=0, co...  4.43 us
    pallas_call x1, Pallas kernels, mixer(): pl.pallas_call(carry_kernel, out_shape=(jax.ShapeDtypeStruct((T, 4 * LANE...  4.35 us
  transfers between devices with their start and end apart: 3, of which 2 were waited for; matrix products, arithmetic and copies ran while one was open for 4% of the time, Pallas kernels for 8%

profile of v1, /device:TPU:1, one launch (start us, length us, event | category | flops | bytes accessed | tf_op | source)
XLA Modules:
  0.0 101.7 jit_solution(14095652740410755030)
XLA Ops:
  0.0 0.8 reshape.99.steps_ref
  0.8 6.0 %ends.1.refs_9_ = bf16[2048,128]{1,0:T(8,128)(2,1)} custom-call(s32[1]{0:T(128)} %bitcast.1.me_ref, f32[64]{0:T(128)S(1)} %reshape.99.steps_ref, bf16[128,256]{1,0:T(8,128)(2,1)} %refs_2_.5, bf16[128,256]{1,0:T(8,128)(2,1)} %refs_3_.5, f32[2,2,16,64]{3,2,1,0:T(8,128)} %refs_0_.5, f32[2,2,16,32]{3,2,1,0:T(8,128)} %refs_1_.5, f32[2,2,16,16,64]{4,3,2,1,0:T(8,128)} %refs_4_.4, ...), custom_call_target="tpu_custom_call" | custom-call | tf_op jit(solution)/shard_map/ends/pallas_call | solution.py:350
  6.8 12.0 %all-to-all-start = ((bf16[64,32,128]{2,1,0:T(8,128)(2,1)}), bf16[64,32,128]{2,1,0:T(8,128)(2,1)S(1)}, u32[]{:S(2)}, u32[]{:S(2)}) async-start(bf16[64,32,128]{2,1,0:T(8,128)(2,1)} %bitcast.3), calls=%async_computation | async-start | bytes 1048576 | tf_op jit(solution)/shard_map/all_to_all | solution.py:359
  18.7 0.0 copy-start
  18.8 0.0 copy-start.1
  18.8 0.0 copy-start.2
  18.8 1.0 copy.33
  19.8 0.8 reshape.103.refs_7_
  20.5 0.8 slice_bitcast_fusion.1
  21.3 0.2 select_reduce_fusion.1
  21.5 0.8 multiply_add_fusion.1
  22.2 0.1 broadcast_add_fusion.1
  22.3 0.1 add.67
  22.4 0.1 add.71
  22.5 0.0 slice-start.2
  22.5 8.4 %local.1 = (f32[128,512]{1,0:T(8,128)}, bf16[128,6144]{1,0:T(8,128)(2,1)}) custom-call(f32[64]{0:T(128)S(1)} %reshape.99.steps_ref, bf16[128,256]{1,0:T(8,128)(2,1)} %refs_2_.5, bf16[128,256]{1,0:T(8,128)(2,1)} %refs_3_.5, f32[2,2,16,64]{3,2,1,0:T(8,128)} %refs_0_.5, f32[2,2,16,32]{3,2,1,0:T(8,128)} %refs_1_.5, f32[2,2,16,16,64]{4,3,2,1,0:T(8,128)} %refs_4_.4, ...), custom_call_target="tpu_custom_call" | custom-call | tf_op jit(solution)/shard_map/local/pallas_call | solution.py:363
  30.9 0.0 all-to-all-done
  30.9 0.0 slice-start
  30.9 0.0 slice-start.1
  30.9 0.0 slice-start.3
  30.9 4.4 %carry.1 = (bf16[128,512]{1,0:T(8,128)(2,1)S(1)}, bf16[1024,2048]{1,0:T(8,128)(2,1)S(1)}) custom-call(s32[1]{0:T(128)} %bitcast.1.me_ref, bf16[2048,128]{1,0:T(8,128)(2,1)S(1)} %bitcast.39, f32[2,2,16,64]{3,2,1,0:T(8,128)} %refs_0_.5, f32[2,2,16,32]{3,2,1,0:T(8,128)} %refs_1_.5, bf16[128,256]{1,0:T(8,128)(2,1)} %refs_2_.5, bf16[128,256]{1,0:T(8,128)(2,1)} %refs_3_.5, ...), custom_call_target="tpu_custom_call" | custom-call | tf_op jit(solution)/shard_map/carry/pallas_call | solution.py:380
  35.3 2.2 %collective-permute-start = (bf16[64,512]{1,0:T(8,128)(2,1)S(1)}, bf16[64,512]{1,0:T(8,128)(2,1)S(1)}, u32[]{:S(2)}, u32[]{:S(2)}) collective-permute-start(bf16[64,512]{1,0:T(8,128)(2,1)S(1)} %get-tuple-element.19), channel_id=1, source_target_pairs={{0,1},{1,0},{2,3},{3,2},{4,5},{5,4},{6,7},{7,6},{8,9},{9,8},{10,11... | collective-permute-start | bytes 196616 | tf_op jit(solution)/shard_map/ppermute | solution.py:516
  37.5 0.9 collective-permute-done.other_ref
  38.4 0.0 copy-done
  38.4 0.0 copy-done.1
  38.4 0.0 copy-done.2
  38.4 1.5 %project.1 = (bf16[64,2048]{1,0:T(8,128)(2,1)S(1)}, bf16[1024,512]{1,0:T(8,128)(2,1)S(1)}) custom-call(s32[1]{0:T(128)} %bitcast.core_ref, bf16[64,512]{1,0:T(8,128)(2,1)S(1)} %get-tuple-element.20.mine_ref, bf16[64,512]{1,0:T(8,128)(2,1)S(1)} %collective-permute-done.other_ref, s32[2,256]{1,0:T(2,128)S(1)} %pad_add_fusion.rows_ref, f32[1,1024]{1,0:T(1,128)S(1)} %bitcast.44, ...), custom_call_target="tpu_custom_call" | custom-call | tf_op jit(solution)/shard_map/project/pallas_call | solution.py:522
  39.9 27.1 %all_to_all.15 = bf16[128,8,512]{2,1,0:T(8,128)(2,1)S(1)} all-to-all(bf16[128,8,512]{2,1,0:T(8,128)(2,1)S(1)} %bitcast.40), channel_id=1, replica_groups=mesh['sp_0'=4,'sp_1'=4,'sp_2'=4,'tp'=2] {'sp_0','sp_1','sp_2','tp'}, dimensions={0} | all-to-all | bytes 2097152 | tf_op jit(solution)/shard_map/all_to_all | solution.py:536
  67.1 0.0 slice-done.2
  67.1 0.0 slice-done
  67.1 0.0 slice-done.1
  67.1 0.0 slice-done.3
  67.1 0.0 copy-start.3
  67.1 9.2 %experts.1 = bf16[1024,512]{1,0:T(8,128)(2,1)} custom-call(bf16[1024,512]{1,0:T(8,128)(2,1)S(1)} %bitcast.37, bf16[2048,1408]{1,0:T(8,128)(2,1)S(1)} %bitcast.33, bf16[2048,1408]{1,0:T(8,128)(2,1)S(1)} %bitcast.36, bf16[1408,2048]{1,0:T(8,128)(2,1)} %bitcast.45), custom_call_target="tpu_custom_call" | custom-call | tf_op jit(solution)/shard_map/experts/pallas_call | solution.py:539
  76.4 4.4 %all-to-all-start.2 = ((bf16[128,8,512]{2,1,0:T(8,128)(2,1)}), bf16[128,8,512]{2,1,0:T(8,128)(2,1)S(1)}, u32[]{:S(2)}, u32[]{:S(2)}) async-start(bf16[128,8,512]{2,1,0:T(8,128)(2,1)} %bitcast.18), calls=%async_computation.2 | async-start | bytes 2097152 | tf_op jit(solution)/shard_map/all_to_all | solution.py:536
  80.8 0.1 copy.34
  80.9 0.0 copy-done.3
  80.9 0.1 copy.35.weights_ref
  81.0 19.1 %all-to-all-done.2 = bf16[128,8,512]{2,1,0:T(8,128)(2,1)S(1)} async-done(((bf16[128,8,512]{2,1,0:T(8,128)(2,1)}), bf16[128,8,512]{2,1,0:T(8,128)(2,1)S(1)}, u32[]{:S(2)}, u32[]{:S(2)}) %all-to-all-start.2) | async-done | bytes 1048608 | tf_op jit(solution)/shard_map/all_to_all | solution.py:536
  100.1 1.5 %combine.1 = bf16[64,2048]{1,0:T(8,128)(2,1)} custom-call(bf16[1024,512]{1,0:T(8,128)(2,1)S(1)} %bitcast.38, s32[256,2]{1,0:T(8,128)S(1)} %bitcast.41, f32[64,2]{1,0:T(8,128)S(1)} %copy.35.weights_ref, bf16[64,2048]{1,0:T(8,128)(2,1)S(1)} %get-tuple-element.16.hidden_ref), custom_call_target="tpu_custom_call" | custom-call | tf_op jit(solution)/shard_map/combine/pallas_call | solution.py:553
  (5 shorter events, 0.0 us)
Async XLA Ops:
  6.8 24.1 %all-to-all-start = ((bf16[64,32,128]{2,1,0:T(8,128)(2,1)}), bf16[64,32,128]{2,1,0:T(8,128)(2,1)S(1)}, u32[]{:S(2)}, u32[]{:S(2)}) async-start(bf16[64,32,128]{2,1,0:T(8,128)(2,1)} %bitcast.3), calls=%async_computation | async-start | bytes 1048576 | tf_op jit(solution)/shard_map/all_to_all | solution.py:359
  18.7 19.7 %copy-start = (bf16[64,2048]{1,0:T(8,128)(2,1)S(1)}, bf16[64,2048]{1,0:T(8,128)(2,1)}, u32[]{:S(2)}) copy-start(bf16[64,2048]{1,0:T(8,128)(2,1)} %residual_ref.1) | copy-start | bytes 786436
  18.8 19.7 %copy-start.1 = (f32[2048]{0:T(1024)S(1)}, f32[2048]{0:T(1024)}, u32[]{:S(2)}) copy-start(f32[2048]{0:T(1024)} %param.36) | copy-start | bytes 24580
  18.8 19.7 %copy-start.2 = (f32[1024]{0:T(1024)S(1)}, f32[1024]{0:T(1024)}, u32[]{:S(2)}) copy-start(f32[1024]{0:T(1024)} %param.34) | copy-start | bytes 12292
  22.5 44.6 %slice-start.2 = ((s8[5767168]{0:T(1024)(128)(4,1)}), s8[1572864]{0:T(1024)(128)(4,1)S(1)}, s32[]{:S(2)}) async-start(s8[5767168]{0:T(1024)(128)(4,1)} %bitcast.34), calls=%async_computation.5 | async-start | bytes 3145728
  30.9 36.1 %slice-start = ((s8[5767168]{0:T(1024)(128)(4,1)}), s8[4194304]{0:T(1024)(128)(4,1)S(1)}, s32[]{:S(2)}) async-start(s8[5767168]{0:T(1024)(128)(4,1)} %bitcast.31), calls=%async_computation.3 | async-start | bytes 8388608
  30.9 36.1 %slice-start.1 = ((s8[5767168]{0:T(1024)(128)(4,1)}), s8[1572864]{0:T(1024)(128)(4,1)S(1)}, s32[]{:S(2)}) async-start(s8[5767168]{0:T(1024)(128)(4,1)} %bitcast.31), calls=%async_computation.4 | async-start | bytes 3145728
  30.9 36.1 %slice-start.3 = ((s8[5767168]{0:T(1024)(128)(4,1)}), s8[4194304]{0:T(1024)(128)(4,1)S(1)}, s32[]{:S(2)}) async-start(s8[5767168]{0:T(1024)(128)(4,1)} %bitcast.34), calls=%async_computation.6 | async-start | bytes 8388608
  35.3 3.1 %collective-permute-start = (bf16[64,512]{1,0:T(8,128)(2,1)S(1)}, bf16[64,512]{1,0:T(8,128)(2,1)S(1)}, u32[]{:S(2)}, u32[]{:S(2)}) collective-permute-start(bf16[64,512]{1,0:T(8,128)(2,1)S(1)} %get-tuple-element.19), channel_id=1, source_target_pairs={{0,1},{1,0},{2,3},{3,2},{4,5},{5,4},{6,7},{7,6},{8,9},{9,8},{10,11... | collective-permute-start | bytes 196616 | tf_op jit(solution)/shard_map/ppermute | solution.py:516
  67.1 13.8 %copy-start.3 = (f32[64,2]{0,1:T(2,128)S(1)}, f32[64,2]{0,1:T(2,128)}, u32[]{:S(2)}) copy-start(f32[64,2]{0,1:T(2,128)} %param.38) | copy-start | bytes 1540
  76.4 23.8 %all-to-all-start.2 = ((bf16[128,8,512]{2,1,0:T(8,128)(2,1)}), bf16[128,8,512]{2,1,0:T(8,128)(2,1)S(1)}, u32[]{:S(2)}, u32[]{:S(2)}) async-start(bf16[128,8,512]{2,1,0:T(8,128)(2,1)} %bitcast.18), calls=%async_computation.2 | async-start | bytes 2097152 | tf_op jit(solution)/shard_map/all_to_all | solution.py:536

commit v2 on v1

--- a/solution.py
+++ b/solution.py
@@ -28,11 +28,6 @@
     for copy in copies:
         copy.start()
     return copies
-
-
-def fetch(sources, buffers, sems):
-    for copy in started(sources, buffers, sems):
-        copy.wait()
 
 
 def lane_ids(shape):
@@ -97,7 +92,7 @@
         re, im = [], []
         for h in range(parts):
             g = r + rows * h
-            step = steps_ref[(d * 2 + which) * 16 + g]
+            step = steps_ref[d, which, g]
             gr, gi = fr[g : g + 1] * step, fi[g : g + 1] * step
             br, bi = in_ref[d, 0, g], in_ref[d, 1, g]
             re.append(gr * br - gi * bi)
@@ -114,24 +109,33 @@
     return jnp.transpose(jnp.concatenate([both, both], axis=0))
 
 
-def load_pushes(steps_ref, u_refs, pole_refs, in_refs, forget_t, scr):
+def load_pushes(copies, buffers, scr):
+    wu_ref, nu_ref, wp_ref, np_ref, wi_ref, ni_ref, forget_ref, steps_ref = buffers
+    copies[6].wait()
+    forget_t = forget_columns(forget_ref)
     kept = jnp.exp(-forget_t)
-    turns = []
+    sets = ((WIDE, wu_ref, wp_ref, wi_ref), (NARROW, nu_ref, np_ref, ni_ref))
     for d in range(2):
-        for which, kind in ((0, WIDE), (1, NARROW)):
-            re_ref, im_ref, e_ref = scr[(d * 2 + which) * 3 : (d * 2 + which) * 3 + 3]
+        for which in range(2):
+            k = d * 2 + which
+            kind = sets[which][0]
+            re_ref, im_ref, e_ref = scr[3 * k : 3 * k + 3]
             if kind is NARROW:
                 for ref in (re_ref, im_ref, e_ref):
                     ref[...] = jnp.zeros((8 * T, LANES), F32)
             for r in range(kind[0]):
-                e_ref[pl.ds(r, T, stride=8), :] = spread(kept, (d * 2 + which) * 16, r, kind)
+                e_ref[pl.ds(r, T, stride=8), :] = spread(kept, k * 16, r, kind)
+    for k in (0, 1, 2, 3, 4, 5, 7):
+        copies[k].wait()
+    turns = []
+    for d in range(2):
+        for which, (kind, u_ref, poles_ref, in_ref) in enumerate(sets):
+            k = d * 2 + which
+            re_ref, im_ref, _ = scr[3 * k : 3 * k + 3]
             turns.append(
-                push_into(
-                    steps_ref, which, d, u_refs[which][...], pole_refs[which], in_refs[which],
-                    kind, re_ref, im_ref,
-                )
+                push_into(steps_ref, which, d, u_ref[...], poles_ref, in_ref, kind, re_ref, im_ref)
             )
-    return turns
+    return turns, forget_t
 
 
 def three_terms(x):
@@ -140,14 +144,9 @@
     return hi, mid, x - hi - mid
 
 
-def ends_kernel(me_ref, steps_ref, *refs):
-    sources, send_ref, buffers, sems, scr = refs[:7], refs[7], refs[8:15], refs[15], refs[16:]
-    fetch(sources, buffers, sems)
-    wu_ref, nu_ref, wp_ref, np_ref, wi_ref, ni_ref, forget_ref = buffers
-    forget_t = forget_columns(forget_ref)
-    turns = load_pushes(
-        steps_ref, (wu_ref, nu_ref), (wp_ref, np_ref), (wi_ref, ni_ref), forget_t, scr
-    )
+def ends_kernel(me_ref, *refs):
+    sources, send_ref, buffers, sems, scr = refs[:8], refs[8], refs[9:17], refs[17], refs[18:]
+    turns, forget_t = load_pushes(started(sources, buffers, sems), buffers, scr)
 
     def step(t, state):
         new = []
@@ -191,15 +190,12 @@
     return side_by_side(out_ref[d, 0], r, kind), side_by_side(out_ref[d, 1], r, kind)
 
 
-def local_kernel(steps_ref, *refs):
-    sources, results, buffers = refs[:9], refs[10:12], refs[12:21]
-    sems, y_ref, decay_ref, out_sems, scr = refs[21], refs[22], refs[23], refs[24], refs[25:]
-    fetch(sources, buffers, sems)
-    wu_ref, nu_ref, wp_ref, np_ref, wi_ref, ni_ref, forget_ref, wo_ref, no_ref = buffers
-    turns = load_pushes(
-        steps_ref, (wu_ref, nu_ref), (wp_ref, np_ref), (wi_ref, ni_ref),
-        forget_columns(forget_ref), scr,
-    )
+def local_kernel(*refs):
+    sources, results, buffers, sems = refs[:10], refs[11:13], refs[13:23], refs[23]
+    y_ref, decay_ref, out_sems, scr = refs[24], refs[25], refs[26], refs[27:]
+    copies = started(sources, buffers, sems)
+    turns, _ = load_pushes(copies, buffers[:8], scr)
+    wo_ref, no_ref = buffers[8:]
     prods = scr[12:]
 
     def step(t, state):
@@ -222,6 +218,8 @@
 
     zero = jnp.zeros((8, LANES), F32)
     lax.fori_loop(0, T, step, ((zero, zero, zero + 1.0, zero),) * 4, unroll=4)
+    copies[8].wait()
+    copies[9].wait()
     for which, (kind, out_ref) in enumerate(((WIDE, wo_ref), (NARROW, no_ref))):
         total = jnp.zeros((T, 2 * LANES), F32)
         for d in range(2):
@@ -238,7 +236,8 @@
                 first = ((d * 12) + which * 8 + r) * 2 * LANES
                 decay_ref[:, first : first + 2 * LANES] = decay.astype(BF16)
         y_ref[:, which * 2 * LANES : (which + 1) * 2 * LANES] = total
-    fetch((y_ref, decay_ref), results, out_sems)
+    for copy in started((y_ref, decay_ref), results, out_sems):
+        copy.wait()
 
 
 def carry_kernel(me_ref, got_ref, *refs):
@@ -305,11 +304,12 @@
         active = 0.5 * shaped * (1.0 + jnp.tanh(inner))
         hi = active.astype(BF16)
         lo = (active - hi.astype(F32)).astype(BF16)
-        line = gate_ref[which].astype(F32)
-        ids = lane_ids(line.shape) // 16
-        gate = jnp.concatenate(
-            [jnp.where(ids == g, line, 0.0).astype(BF16) for g in range(16)], axis=0
-        )
+        spread_out = jnp.where(
+            lane_ids((16, 256)) % 16 == lax.broadcasted_iota(jnp.int32, (16, 256), 0), 1.0, 0.0
+        ).astype(BF16)
+        gate = jnp.dot(gate_ref[which], spread_out, preferred_element_type=F32)
+        own = lax.broadcasted_iota(jnp.int32, (256, 256), 0) // 16 == lane_ids((256, 256)) // 16
+        gate = jnp.where(own, gate, 0.0).astype(BF16)
         mixed = jnp.dot(hi, gate, preferred_element_type=F32) + jnp.dot(
             lo, gate, preferred_element_type=F32
         )
@@ -328,13 +328,17 @@
 
 
 def fetched(arrays):
-    return [pltpu.VMEM(a.shape, a.dtype) for a in arrays] + [
-        pltpu.SemaphoreType.DMA((len(arrays),))
-    ]
+    return [
+        (pltpu.SMEM if a.shape == (2, 2, 16) else pltpu.VMEM)(a.shape, a.dtype) for a in arrays
+    ] + [pltpu.SemaphoreType.DMA((len(arrays),))]
 
 
 def far(arrays):
     return tuple(pltpu.with_memory_space_constraint(a, pltpu.HBM) for a in arrays)
+
+
+def cost(us):
+    return pl.CostEstimate(flops=int(us * 1e9), bytes_accessed=int(us * 1e6), transcendentals=0)
 
 
 def grant(mib):
@@ -344,18 +348,18 @@
 def mixer(me, wide_u, narrow_u, wide_p, narrow_p, steps, forget, wide_in, narrow_in, wide_out,
           narrow_out, skip, gate, out_proj):
     blocks = lax.axis_size(SP)
-    steps = steps.reshape(-1)
     forget = forget.reshape(-1, T)
-    shared = far((wide_u, narrow_u, wide_p, narrow_p, wide_in, narrow_in, forget))
+    shared = far((wide_u, narrow_u, wide_p, narrow_p, wide_in, narrow_in, forget, steps))
     send = pl.pallas_call(
         ends_kernel,
         out_shape=jax.ShapeDtypeStruct((blocks * 32, LANES), BF16),
-        in_specs=[SMEM, SMEM] + [HBM] * 7,
+        in_specs=[SMEM] + [HBM] * 8,
         out_specs=VMEM,
         scratch_shapes=fetched(shared) + [column(T)] * 12,
         compiler_params=grant(20),
+        cost_estimate=cost(6),
         name="ends",
-    )(me, steps, *shared)
+    )(me, *shared)
     got = lax.all_to_all(
         send.reshape(blocks, 32, LANES), SP, split_axis=0, concat_axis=0, tiled=True
     )
@@ -366,14 +370,15 @@
             pltpu.HBM((T, 4 * LANES), F32),
             pltpu.HBM((T, 24 * 2 * LANES), BF16),
         ),
-        in_specs=[SMEM] + [HBM] * 10,
+        in_specs=[HBM] * 11,
         out_specs=(HBM, HBM),
         scratch_shapes=fetched(sources)
         + [pltpu.VMEM((T, 4 * LANES), F32), pltpu.VMEM((T, 24 * 2 * LANES), BF16)]
         + [pltpu.SemaphoreType.DMA((2,))] + [column(T)] * 20,
         compiler_params=grant(24),
+        cost_estimate=cost(8),
         name="local",
-    )(steps, *sources, send)
+    )(*sources, *far((send,)))
     sources = far(
         (wide_p, narrow_p, wide_u, narrow_u, wide_out, narrow_out, skip, gate, y, decay, out_proj)
     )
@@ -388,15 +393,42 @@
         scratch_shapes=[pltpu.VMEM(a.shape, a.dtype) for a in sources[:10]]
         + [pltpu.SemaphoreType.DMA((11,))]
         + [pltpu.VMEM((blocks * 32, LANES), F32)] + [column(blocks)] * 4,
-        compiler_params=grant(20),
+        compiler_params=grant(16),
+        cost_estimate=cost(5),
         name="carry",
     )(me, got.reshape(-1, LANES), *sources)
 
 
+def places(routes):
+    n = routes.shape[1]
+    flat = jnp.concatenate([routes, routes], axis=1).astype(F32)
+    line = [flat[k : k + 1] for k in range(2)]
+    first = lax.broadcasted_iota(jnp.int32, (2 * n, 2 * n), 0) == 0
+    table = jnp.transpose(jnp.where(first, line[0], line[1]))
+    lanes, rows = lane_ids((n, 2 * n)), lax.broadcasted_iota(jnp.int32, (n, 2 * n), 0)
+    wide = [jnp.broadcast_to(table[:n, k : k + 1], (n, 2 * n)) for k in range(2)]
+    across, down = [], []
+    for k in range(2):
+        over, under = 0.0, 0.0
+        for o in range(2):
+            over += jnp.where((rows < lanes % n) & (wide[o] == line[k]), 1.0, 0.0)
+            under += jnp.where((lanes < rows) & (wide[k] == line[o]), 1.0, 0.0)
+        at = line[k] * 8.0 + jnp.sum(over, axis=0, keepdims=True) + 2.0 * (lanes[:1] // n)
+        across.append(jnp.concatenate([at, at + 4.0], axis=1).astype(jnp.int32))
+        at = table[:n, k : k + 1] * 8.0 + jnp.sum(under, axis=1, keepdims=True)
+        down.append(jnp.concatenate([at + 2.0 * q for q in range(4)], axis=0).astype(jnp.int32))
+    return across, down
+
+
 def project_kernel(
-    core_ref, mine_ref, other_ref, rows_ref, gain_ref, ffn_ref, residual_ref, proj_ref, hidden_ref,
-    send_ref,
+    core_ref, mine_ref, other_ref, routes_ref, gain_ref, ffn_ref, residual_ref, proj_ref,
+    hidden_ref, send_ref, cols_ref,
 ):
+    across, down = places(routes_ref[...])
+    shape = cols_ref.shape
+    cols_ref[...] = jnp.where(
+        lane_ids(shape) == 0, jnp.broadcast_to(down[0], shape), jnp.broadcast_to(down[1], shape)
+    )
     swap = core_ref[0] == 1
     mine, other = mine_ref[...].astype(F32), other_ref[...].astype(F32)
     first, second = jnp.where(swap, other, mine), jnp.where(swap, mine, other)
@@ -417,7 +449,7 @@
     size = stacked.shape[0]
     for b in range(send_ref.shape[0] // size):
         ids = lax.broadcasted_iota(jnp.int32, (size, size), 0) + b * size
-        hit = (ids == rows_ref[0:1, :]) | (ids == rows_ref[1:2, :])
+        hit = (ids == across[0]) | (ids == across[1])
         pick = jnp.where(hit, 1.0, 0.0).astype(BF16)
         send_ref[b * size : (b + 1) * size, :] = jnp.dot(
             pick, stacked, preferred_element_type=F32
@@ -484,25 +516,13 @@
     out_ref[...] = result.astype(BF16)
 
 
-def ranks(routes):
-    rows = routes.shape[0]
-    earlier = jnp.arange(rows)[None, :] < jnp.arange(rows)[:, None]
-    out = []
-    for k in range(2):
-        same = sum(
-            (routes[:, k][:, None] == routes[:, o][None, :]).astype(jnp.int32) for o in range(2)
-        )
-        out.append(jnp.sum(jnp.where(earlier, same, 0), axis=1))
-    return out
-
-
 def local(
     wide_inputs, narrow_inputs, wide_poles, narrow_poles, step_sizes, forget, wide_in_map,
     narrow_in_map, wide_out_map, narrow_out_map, skip_weight, gate_mix, residual, mixer_gain,
     out_proj, ffn_gain, routes, route_weights, gate_proj, up_proj, down_proj,
 ):
     me = lax.axis_index(SP).astype(jnp.int32).reshape(1)
-    gate_rows = jnp.transpose(gate_mix, (0, 2, 1, 3)).reshape(2, 16, 256)
+    gate_rows = gate_mix.reshape(2, 256, 16)
     set_out, near_proj = mixer(
         me, wide_inputs, narrow_inputs, wide_poles, narrow_poles, step_sizes, forget, wide_in_map,
         narrow_in_map, wide_out_map, narrow_out_map, skip_weight, gate_rows, out_proj,
@@ -515,22 +535,20 @@
     other = lax.dynamic_index_in_dim(halves, 1 - core, 0, keepdims=False)
     other = lax.ppermute(other, "tp", [(0, 1), (1, 0)])
     experts = lax.axis_size(SP) * lax.axis_size("tp")
-    quarters = jnp.repeat(jnp.arange(4, dtype=jnp.int32) * 2, rows)
-    places = jnp.stack(
-        [jnp.tile(routes[:, k] * 8 + rank, 4) + quarters for k, rank in enumerate(ranks(routes))]
-    )
-    hidden1, send = pl.pallas_call(
+    hidden1, send, cols = pl.pallas_call(
         project_kernel,
         out_shape=(
             jax.ShapeDtypeStruct((rows, width), BF16),
             jax.ShapeDtypeStruct((experts * 8, width // 4), BF16),
+            jax.ShapeDtypeStruct((4 * rows, LANES), jnp.int32),
         ),
         in_specs=[SMEM] + [VMEM] * 7,
-        out_specs=(VMEM, VMEM),
+        out_specs=(VMEM, VMEM, VMEM),
         compiler_params=grant(12),
+        cost_estimate=cost(2),
         name="project",
     )(
-        core.reshape(1), mine, other, places, mixer_gain.reshape(1, -1), ffn_gain.reshape(1, -1),
+        core.reshape(1), mine, other, routes.T, mixer_gain.reshape(1, -1), ffn_gain.reshape(1, -1),
         residual, near_proj,
     )
     exchange = lambda x: lax.all_to_all(
@@ -548,6 +566,7 @@
             pltpu.SemaphoreType.DMA,
         ],
         compiler_params=grant(20),
+        cost_estimate=cost(9),
         name="experts",
     )(exchange(send), gate_proj[0], up_proj[0], *far((down_proj[0],)))
     return pl.pallas_call(
@@ -556,8 +575,9 @@
         in_specs=[VMEM] * 4,
         out_specs=VMEM,
         compiler_params=grant(12),
+        cost_estimate=cost(2),
         name="combine",
-    )(exchange(done), places.T, route_weights, hidden1)
+    )(exchange(done), cols, route_weights, hidden1)
 
 
 def solution(mesh):

time: 102 us -> 96.7 us (0.948)
  waiting for transfers between devices: 20 us -> 24.6 us
  blocking collectives: 27.1 us -> 22.7 us
  local copies, waits for them, and re-layouts: 3.71 us -> 0.16 us
  other arithmetic: 1.03 us -> 0.01 us
    all_to_all x1, waiting for transfers between devices: 0.04 us -> 4.48 us  [mixer(): lax.all_to_all(send.reshape(blocks, 32, LANES), SP, split_axis=0, concat_...]
    all_to_all x1, blocking collectives: 27.1 us -> 22.7 us  [local(): lax.all_to_all(x.reshape(experts, 8, width // 4), SP_TP, split_axis=0, co...]
    reshape x2 -> x0, local copies, waits for them, and re-layouts: 1.52 us -> none  [the longest x1 0.76 us: mixer(): steps = steps.reshape(-1)]
  transfers between devices with their start and end apart: 3 -> 3, of which waited for: 2 -> 3; matrix products, arithmetic and copies ran while one was open for 4% -> 0% of each run, Pallas kernels for 8% -> 8%
where the time goes in v2:
time: 96.7 us; the launch traced here: 96.4 us
  Pallas kernels  30.1 us (31%)
  waiting for transfers between devices  24.6 us (25%)
  blocking collectives  22.7 us (23%)
  starting transfers between devices  18.6 us (19%)
    all_to_all x1, blocking collectives, local(): lax.all_to_all(x.reshape(experts, 8, width // 4), SP_TP, split_axis=0, co...  22.7 us
    all_to_all x1, waiting for transfers between devices, local(): lax.all_to_all(x.reshape(experts, 8, width // 4), SP_TP, split_axis=0, co...  19.2 us
    all_to_all x1, starting transfers between devices, mixer(): lax.all_to_all(send.reshape(blocks, 32, LANES), SP, split_axis=0, concat_...  12 us
    pallas_call x1, Pallas kernels, local(): pl.pallas_call(experts_kernel, out_shape=jax.ShapeDtypeStruct((experts *...  9.25 us
    pallas_call x1, Pallas kernels, mixer(): pl.pallas_call(local_kernel, out_shape=(pltpu.HBM((T, 4 * LANES), F32), p...  7.66 us
    pallas_call x1, Pallas kernels, mixer(): pl.pallas_call(ends_kernel, out_shape=jax.ShapeDtypeStruct((blocks * 32,...  5.6 us
    pallas_call x1, Pallas kernels, mixer(): pl.pallas_call(carry_kernel, out_shape=(jax.ShapeDtypeStruct((T, 4 * LANE...  4.49 us
    all_to_all x1, waiting for transfers between devices, mixer(): lax.all_to_all(send.reshape(blocks, 32, LANES), SP, split_axis=0, concat_...  4.48 us
  transfers between devices with their start and end apart: 3, of which 3 were waited for; matrix products, arithmetic and copies ran while one was open for 0% of the time, Pallas kernels for 8%

profile of v2, /device:TPU:1, one launch (start us, length us, event | category | flops | bytes accessed | tf_op | source)
XLA Modules:
  0.0 96.4 jit_solution(6061151193948430292)
XLA Ops:
  0.0 5.6 %ends.1.refs_10_ = bf16[2048,128]{1,0:T(8,128)(2,1)} custom-call(s32[1]{0:T(128)} %bitcast.1.me_ref, bf16[128,256]{1,0:T(8,128)(2,1)} %refs_2_.5, bf16[128,256]{1,0:T(8,128)(2,1)} %refs_3_.5, f32[2,2,16,64]{3,2,1,0:T(8,128)} %refs_0_.5, f32[2,2,16,32]{3,2,1,0:T(8,128)} %refs_1_.5, f32[2,2,16,16,64]{4,3,2,1,0:T(8,128)} %refs_4_.4, ...), custom_call_target="tpu_custom_call" | custom-call | flops 6000000000 | bytes 6000000 | tf_op jit(solution)/shard_map/ends/pallas_call | solution.py:353
  5.6 12.0 %all-to-all-start = ((bf16[64,32,128]{2,1,0:T(8,128)(2,1)}), bf16[64,32,128]{2,1,0:T(8,128)(2,1)S(1)}, u32[]{:S(2)}, u32[]{:S(2)}) async-start(bf16[64,32,128]{2,1,0:T(8,128)(2,1)} %bitcast.3), calls=%async_computation | async-start | bytes 1048576 | tf_op jit(solution)/shard_map/all_to_all | solution.py:363
  17.6 7.7 %local.1 = (f32[128,512]{1,0:T(8,128)}, bf16[128,6144]{1,0:T(8,128)(2,1)}) custom-call(bf16[128,256]{1,0:T(8,128)(2,1)} %refs_2_.5, bf16[128,256]{1,0:T(8,128)(2,1)} %refs_3_.5, f32[2,2,16,64]{3,2,1,0:T(8,128)} %refs_0_.5, f32[2,2,16,32]{3,2,1,0:T(8,128)} %refs_1_.5, f32[2,2,16,16,64]{4,3,2,1,0:T(8,128)} %refs_4_.4, f32[2,2,16,16,32]{4,3,2,1,0:T(8,128)} %refs_5_.4, ...), custom_call_target="tpu_custom_call" | custom-call | flops 8000000000 | bytes 8000000 | tf_op jit(solution)/shard_map/local/pallas_call | solution.py:367
  25.3 4.5 %all-to-all-done = bf16[64,32,128]{2,1,0:T(8,128)(2,1)S(1)} async-done(((bf16[64,32,128]{2,1,0:T(8,128)(2,1)}), bf16[64,32,128]{2,1,0:T(8,128)(2,1)S(1)}, u32[]{:S(2)}, u32[]{:S(2)}) %all-to-all-start) | async-done | bytes 524320 | tf_op jit(solution)/shard_map/all_to_all | solution.py:363
  29.7 0.0 slice-start
  29.7 0.0 slice-start.2
  29.7 0.0 copy-start
  29.7 0.0 copy-start.1
  29.8 0.0 copy-start.2
  29.8 0.0 copy-start.3
  29.8 0.0 slice-start.1
  29.8 0.0 slice-start.3
  29.8 4.5 %carry.1 = (bf16[128,512]{1,0:T(8,128)(2,1)S(1)}, bf16[1024,2048]{1,0:T(8,128)(2,1)S(1)}) custom-call(s32[1]{0:T(128)} %bitcast.1.me_ref, bf16[2048,128]{1,0:T(8,128)(2,1)S(1)} %bitcast.24, f32[2,2,16,64]{3,2,1,0:T(8,128)} %refs_0_.5, f32[2,2,16,32]{3,2,1,0:T(8,128)} %refs_1_.5, bf16[128,256]{1,0:T(8,128)(2,1)} %refs_2_.5, bf16[128,256]{1,0:T(8,128)(2,1)} %refs_3_.5, ...), custom_call_target="tpu_custom_call" | custom-call | flops 5000000000 | bytes 5000000 | tf_op jit(solution)/shard_map/carry/pallas_call | solution.py:385
  34.3 2.2 %collective-permute-start = (bf16[64,512]{1,0:T(8,128)(2,1)S(1)}, bf16[64,512]{1,0:T(8,128)(2,1)S(1)}, u32[]{:S(2)}, u32[]{:S(2)}) collective-permute-start(bf16[64,512]{1,0:T(8,128)(2,1)S(1)} %get-tuple-element.19), channel_id=1, source_target_pairs={{0,1},{1,0},{2,3},{3,2},{4,5},{5,4},{6,7},{7,6},{8,9},{9,8},{10,11... | collective-permute-start | bytes 196616 | tf_op jit(solution)/shard_map/ppermute | solution.py:536
  36.6 0.9 collective-permute-done.other_ref
  37.5 0.0 copy-done
  37.5 0.0 copy-done.1
  37.5 0.0 copy-done.2
  37.5 0.0 copy-done.3
  37.5 1.6 %project.1 = (bf16[64,2048]{1,0:T(8,128)(2,1)S(1)}, bf16[1024,512]{1,0:T(8,128)(2,1)S(1)}, s32[256,128]{1,0:T(8,128)S(1)}) custom-call(s32[1]{0:T(128)} %bitcast.core_ref, bf16[64,512]{1,0:T(8,128)(2,1)S(1)} %get-tuple-element.20.mine_ref, bf16[64,512]{1,0:T(8,128)(2,1)S(1)} %collective-permute-done.other_ref, s32[2,64]{1,0:T(2,128)S(1)} %bitcast.34, ...), custom_call_target="tpu_custom_call" | custom-call | flops 2000000000 | bytes 2000000 | tf_op jit(solution)/shard_map/project/pallas_call | solution.py:538
  39.1 22.7 %all_to_all.15 = bf16[128,8,512]{2,1,0:T(8,128)(2,1)S(1)} all-to-all(bf16[128,8,512]{2,1,0:T(8,128)(2,1)S(1)} %bitcast.22), channel_id=1, replica_groups=mesh['sp_0'=4,'sp_1'=4,'sp_2'=4,'tp'=2] {'sp_0','sp_1','sp_2','tp'}, dimensions={0} | all-to-all | bytes 2097152 | tf_op jit(solution)/shard_map/all_to_all | solution.py:554
  61.8 0.0 slice-done
  61.8 0.0 slice-done.2
  61.8 0.0 slice-done.1
  61.8 0.0 slice-done.3
  61.8 0.0 copy-start.4
  61.8 9.2 %experts.1 = bf16[1024,512]{1,0:T(8,128)(2,1)} custom-call(bf16[1024,512]{1,0:T(8,128)(2,1)S(1)} %bitcast.23, bf16[2048,1408]{1,0:T(8,128)(2,1)S(1)} %bitcast.28, bf16[2048,1408]{1,0:T(8,128)(2,1)S(1)} %bitcast.31, bf16[1408,2048]{1,0:T(8,128)(2,1)} %bitcast.35), custom_call_target="tpu_custom_call" | custom-call | flops 8999999488 | bytes 9000000 | tf_op jit(solution)/shard_map/experts/pallas_call | solution.py:557
  71.1 4.4 %all-to-all-start.2 = ((bf16[128,8,512]{2,1,0:T(8,128)(2,1)}), bf16[128,8,512]{2,1,0:T(8,128)(2,1)S(1)}, u32[]{:S(2)}, u32[]{:S(2)}) async-start(bf16[128,8,512]{2,1,0:T(8,128)(2,1)} %bitcast.17), calls=%async_computation.2 | async-start | bytes 2097152 | tf_op jit(solution)/shard_map/all_to_all | solution.py:554
  75.5 0.0 copy-done.4
  75.6 0.1 copy.22.weights_ref
  75.7 19.2 %all-to-all-done.2 = bf16[128,8,512]{2,1,0:T(8,128)(2,1)S(1)} async-done(((bf16[128,8,512]{2,1,0:T(8,128)(2,1)}), bf16[128,8,512]{2,1,0:T(8,128)(2,1)S(1)}, u32[]{:S(2)}, u32[]{:S(2)}) %all-to-all-start.2) | async-done | bytes 1048608 | tf_op jit(solution)/shard_map/all_to_all | solution.py:554
  94.9 1.5 %combine.1 = bf16[64,2048]{1,0:T(8,128)(2,1)} custom-call(bf16[1024,512]{1,0:T(8,128)(2,1)S(1)} %bitcast.21, s32[256,128]{1,0:T(8,128)S(1)} %get-tuple-element.17.cols_ref, f32[64,2]{1,0:T(8,128)S(1)} %copy.22.weights_ref, bf16[64,2048]{1,0:T(8,128)(2,1)S(1)} %get-tuple-element.18.hidden_ref), custom_call_target="tpu_custom_call" | custom-call | flops 2000000000 | bytes 2000000 | tf_op jit(solution)/shard_map/combine/pallas_call | solution.py:572
  (3 shorter events, 0.0 us)
Async XLA Ops:
  5.6 24.1 %all-to-all-start = ((bf16[64,32,128]{2,1,0:T(8,128)(2,1)}), bf16[64,32,128]{2,1,0:T(8,128)(2,1)S(1)}, u32[]{:S(2)}, u32[]{:S(2)}) async-start(bf16[64,32,128]{2,1,0:T(8,128)(2,1)} %bitcast.3), calls=%async_computation | async-start | bytes 1048576 | tf_op jit(solution)/shard_map/all_to_all | solution.py:363
  29.7 32.1 %slice-start = ((s8[5767168]{0:T(1024)(128)(4,1)}), s8[4194304]{0:T(1024)(128)(4,1)S(1)}, s32[]{:S(2)}) async-start(s8[5767168]{0:T(1024)(128)(4,1)} %bitcast.26), calls=%async_computation.3 | async-start | bytes 8388608
  29.7 32.1 %slice-start.2 = ((s8[5767168]{0:T(1024)(128)(4,1)}), s8[4194304]{0:T(1024)(128)(4,1)S(1)}, s32[]{:S(2)}) async-start(s8[5767168]{0:T(1024)(128)(4,1)} %bitcast.29), calls=%async_computation.5 | async-start | bytes 8388608
  29.7 7.7 %copy-start = (bf16[64,2048]{1,0:T(8,128)(2,1)S(1)}, bf16[64,2048]{1,0:T(8,128)(2,1)}, u32[]{:S(2)}) copy-start(bf16[64,2048]{1,0:T(8,128)(2,1)} %residual_ref.1) | copy-start | bytes 786436
  29.7 7.7 %copy-start.1 = (f32[2048]{0:T(1024)S(1)}, f32[2048]{0:T(1024)}, u32[]{:S(2)}) copy-start(f32[2048]{0:T(1024)} %param.36) | copy-start | bytes 24580
  29.8 7.7 %copy-start.2 = (f32[1024]{0:T(1024)S(1)}, f32[1024]{0:T(1024)}, u32[]{:S(2)}) copy-start(f32[1024]{0:T(1024)} %param.34) | copy-start | bytes 12292
  29.8 7.7 %copy-start.3 = (s32[64,2]{0,1:T(2,128)S(1)}, s32[64,2]{0,1:T(2,128)}, u32[]{:S(2)}) copy-start(s32[64,2]{0,1:T(2,128)} %param.37) | copy-start | bytes 1540
  29.8 32.0 %slice-start.1 = ((s8[5767168]{0:T(1024)(128)(4,1)}), s8[1572864]{0:T(1024)(128)(4,1)S(1)}, s32[]{:S(2)}) async-start(s8[5767168]{0:T(1024)(128)(4,1)} %bitcast.26), calls=%async_computation.4 | async-start | bytes 3145728
  29.8 32.0 %slice-start.3 = ((s8[5767168]{0:T(1024)(128)(4,1)}), s8[1572864]{0:T(1024)(128)(4,1)S(1)}, s32[]{:S(2)}) async-start(s8[5767168]{0:T(1024)(128)(4,1)} %bitcast.29), calls=%async_computation.6 | async-start | bytes 3145728
  34.3 3.1 %collective-permute-start = (bf16[64,512]{1,0:T(8,128)(2,1)S(1)}, bf16[64,512]{1,0:T(8,128)(2,1)S(1)}, u32[]{:S(2)}, u32[]{:S(2)}) collective-permute-start(bf16[64,512]{1,0:T(8,128)(2,1)S(1)} %get-tuple-element.19), channel_id=1, source_target_pairs={{0,1},{1,0},{2,3},{3,2},{4,5},{5,4},{6,7},{7,6},{8,9},{9,8},{10,11... | collective-permute-start | bytes 196616 | tf_op jit(solution)/shard_map/ppermute | solution.py:536
  61.8 13.7 %copy-start.4 = (f32[64,2]{0,1:T(2,128)S(1)}, f32[64,2]{0,1:T(2,128)}, u32[]{:S(2)}) copy-start(f32[64,2]{0,1:T(2,128)} %param.38) | copy-start | bytes 1540
  71.1 23.8 %all-to-all-start.2 = ((bf16[128,8,512]{2,1,0:T(8,128)(2,1)}), bf16[128,8,512]{2,1,0:T(8,128)(2,1)S(1)}, u32[]{:S(2)}, u32[]{:S(2)}) async-start(bf16[128,8,512]{2,1,0:T(8,128)(2,1)} %bitcast.17), calls=%async_computation.2 | async-start | bytes 2097152 | tf_op jit(solution)/shard_map/all_to_all | solution.py:554

commit v3 on v2

--- a/solution.py
+++ b/solution.py
@@ -119,10 +119,7 @@
         for which in range(2):
             k = d * 2 + which
             kind = sets[which][0]
-            re_ref, im_ref, e_ref = scr[3 * k : 3 * k + 3]
-            if kind is NARROW:
-                for ref in (re_ref, im_ref, e_ref):
-                    ref[...] = jnp.zeros((8 * T, LANES), F32)
+            e_ref = scr[3 * k + 2]
             for r in range(kind[0]):
                 e_ref[pl.ds(r, T, stride=8), :] = spread(kept, k * 16, r, kind)
     for k in (0, 1, 2, 3, 4, 5, 7):
@@ -191,8 +188,8 @@
 
 
 def local_kernel(*refs):
-    sources, results, buffers, sems = refs[:10], refs[11:13], refs[13:23], refs[23]
-    y_ref, decay_ref, out_sems, scr = refs[24], refs[25], refs[26], refs[27:]
+    sources, (y_ref, decay_ref, factor_ref), buffers = refs[:10], refs[11:14], refs[14:24]
+    sems, scr = refs[24], refs[25:]
     copies = started(sources, buffers, sems)
     turns, _ = load_pushes(copies, buffers[:8], scr)
     wo_ref, no_ref = buffers[8:]
@@ -236,17 +233,18 @@
                 first = ((d * 12) + which * 8 + r) * 2 * LANES
                 decay_ref[:, first : first + 2 * LANES] = decay.astype(BF16)
         y_ref[:, which * 2 * LANES : (which + 1) * 2 * LANES] = total
-    for copy in started((y_ref, decay_ref), results, out_sems):
-        copy.wait()
-
-
-def carry_kernel(me_ref, got_ref, *refs):
-    sources, out_ref, weights_ref, buffers = refs[:11], refs[11], refs[12], refs[13:23]
-    sems, flat, kept = refs[23], refs[24], refs[25:]
+    for k in range(4):
+        cr, ci = turns[k]
+        for _ in range(7):
+            cr, ci = cr * cr - ci * ci, 2.0 * cr * ci
+        factor_ref[16 * k : 16 * k + 8, :], factor_ref[16 * k + 8 : 16 * k + 16, :] = cr, ci
+
+
+def carry_kernel(me_ref, got_ref, y_ref, decay_ref, factor_ref, *refs):
+    sources, out_ref, weights_ref, buffers = refs[:7], refs[7], refs[8], refs[9:15]
+    sems, flat, kept = refs[15], refs[16], refs[17:]
     copies = started(sources, buffers + (weights_ref,), sems)
-    wp_ref, np_ref, wu_ref, nu_ref, wo_ref, no_ref, skip_ref, gate_ref, y_ref, decay_ref = buffers
-    for copy in copies[:2]:
-        copy.wait()
+    wu_ref, nu_ref, wo_ref, no_ref, skip_ref, gate_ref = buffers
     me = me_ref[0]
     blocks = got_ref.shape[0] // 32
     flat[...] = got_ref[...].astype(F32)
@@ -254,18 +252,13 @@
     table = first + pltpu.roll(first, 64, 1) + flat[pl.ds(21, blocks, stride=32), :]
     turns = []
     for d in range(2):
-        for which, (kind, poles_ref) in enumerate(((WIDE, wp_ref), (NARROW, np_ref))):
+        for which, kind in enumerate((WIDE, NARROW)):
             k = d * 2 + which
-            if kind is NARROW:
-                kept[k][...] = jnp.zeros((8 * blocks, LANES), F32)
             for r in range(kind[0]):
                 kept[k][pl.ds(r, blocks, stride=8), :] = spread(table, k * 16, r, kind)
-            pr, pi = poles_ref[d, 0], poles_ref[d, 1]
-            growth = jnp.exp(pr)
-            cr, ci = growth * jnp.cos(pi), growth * jnp.sin(pi)
-            for _ in range(7):
-                cr, ci = cr * cr - ci * ci, 2.0 * cr * ci
-            turns.append((padded8(in_rows(cr, kind)), padded8(in_rows(ci, kind))))
+            turns.append(
+                (factor_ref[16 * k : 16 * k + 8, :], factor_ref[16 * k + 8 : 16 * k + 16, :])
+            )
 
     def step(i, state):
         new = []
@@ -283,7 +276,7 @@
 
     zero = jnp.zeros((8, LANES), F32)
     state = lax.fori_loop(0, blocks, step, ((zero, zero),) * 4, unroll=4)
-    for copy in copies[2:10]:
+    for copy in copies[:6]:
         copy.wait()
     for which, (kind, u_ref, o_ref) in enumerate(((WIDE, wu_ref, wo_ref), (NARROW, nu_ref, no_ref))):
         span = slice(which * 2 * LANES, (which + 1) * 2 * LANES)
@@ -314,7 +307,7 @@
             lo, gate, preferred_element_type=F32
         )
         out_ref[:, span] = (active * jax.nn.sigmoid(mixed)).astype(BF16)
-    copies[10].wait()
+    copies[6].wait()
 
 
 SMEM = pl.BlockSpec(memory_space=pltpu.SMEM)
@@ -331,6 +324,10 @@
     return [
         (pltpu.SMEM if a.shape == (2, 2, 16) else pltpu.VMEM)(a.shape, a.dtype) for a in arrays
     ] + [pltpu.SemaphoreType.DMA((len(arrays),))]
+
+
+def near(arrays):
+    return tuple(pltpu.with_memory_space_constraint(a, pltpu.VMEM) for a in arrays)
 
 
 def far(arrays):
@@ -364,23 +361,22 @@
         send.reshape(blocks, 32, LANES), SP, split_axis=0, concat_axis=0, tiled=True
     )
     sources = shared + far((wide_out, narrow_out))
-    y, decay = pl.pallas_call(
+    y, decay, factors = pl.pallas_call(
         local_kernel,
         out_shape=(
-            pltpu.HBM((T, 4 * LANES), F32),
-            pltpu.HBM((T, 24 * 2 * LANES), BF16),
+            pltpu.VMEM((T, 4 * LANES), F32),
+            pltpu.VMEM((T, 24 * 2 * LANES), BF16),
+            pltpu.VMEM((64, LANES), F32),
         ),
         in_specs=[HBM] * 11,
-        out_specs=(HBM, HBM),
-        scratch_shapes=fetched(sources)
-        + [pltpu.VMEM((T, 4 * LANES), F32), pltpu.VMEM((T, 24 * 2 * LANES), BF16)]
-        + [pltpu.SemaphoreType.DMA((2,))] + [column(T)] * 20,
+        out_specs=(VMEM, VMEM, VMEM),
+        scratch_shapes=fetched(sources) + [column(T)] * 20,
         compiler_params=grant(24),
         cost_estimate=cost(8),
         name="local",
     )(*sources, *far((send,)))
     sources = far(
-        (wide_p, narrow_p, wide_u, narrow_u, wide_out, narrow_out, skip, gate, y, decay, out_proj)
+        (wide_u, narrow_u, wide_out, narrow_out, skip, gate, out_proj)
     )
     return pl.pallas_call(
         carry_kernel,
@@ -388,15 +384,15 @@
             jax.ShapeDtypeStruct((T, 4 * LANES), BF16),
             jax.ShapeDtypeStruct(out_proj.shape, BF16),
         ),
-        in_specs=[SMEM, VMEM] + [HBM] * 11,
+        in_specs=[SMEM] + [VMEM] * 4 + [HBM] * 7,
         out_specs=(VMEM, VMEM),
-        scratch_shapes=[pltpu.VMEM(a.shape, a.dtype) for a in sources[:10]]
-        + [pltpu.SemaphoreType.DMA((11,))]
+        scratch_shapes=[pltpu.VMEM(a.shape, a.dtype) for a in sources[:6]]
+        + [pltpu.SemaphoreType.DMA((7,))]
         + [pltpu.VMEM((blocks * 32, LANES), F32)] + [column(blocks)] * 4,
         compiler_params=grant(16),
         cost_estimate=cost(5),
         name="carry",
-    )(me, got.reshape(-1, LANES), *sources)
+    )(me, got.reshape(-1, LANES), *near((y, decay, factors)), *sources)
 
 
 def places(routes):
@@ -508,11 +504,13 @@
     got = got_ref[...]
     result = hidden_ref[...].astype(F32)
     ids = lax.broadcasted_iota(jnp.int32, (4 * rows, size), 1)
+    pick = jnp.concatenate(
+        [jnp.where(ids == cols_ref[:, k : k + 1], 1.0, 0.0).astype(BF16) for k in range(2)], axis=0
+    )
+    both = jnp.dot(pick, got, preferred_element_type=F32)
     for k in range(2):
-        pick = jnp.where(ids == cols_ref[:, k : k + 1], 1.0, 0.0).astype(BF16)
-        taken = jnp.dot(pick, got, preferred_element_type=F32)
-        taken = jnp.concatenate([taken[q * rows : (q + 1) * rows] for q in range(4)], axis=1)
-        result = result + (w[:, k : k + 1] / total) * taken
+        parts = [both[(4 * k + q) * rows : (4 * k + q + 1) * rows] for q in range(4)]
+        result = result + (w[:, k : k + 1] / total) * jnp.concatenate(parts, axis=1)
     out_ref[...] = result.astype(BF16)
 
 
@@ -545,7 +543,7 @@
         in_specs=[SMEM] + [VMEM] * 7,
         out_specs=(VMEM, VMEM, VMEM),
         compiler_params=grant(12),
-        cost_estimate=cost(2),
+        cost_estimate=cost(60),
         name="project",
     )(
         core.reshape(1), mine, other, routes.T, mixer_gain.reshape(1, -1), ffn_gain.reshape(1, -1),

time: 96.7 us -> 95.7 us (0.990)
  Pallas kernels: 30.1 us -> 27.9 us
  waiting for transfers between devices: 24.6 us -> 25.8 us
    all_to_all x1, waiting for transfers between devices: 4.48 us -> 5.63 us  [mixer(): lax.all_to_all(send.reshape(blocks, 32, LANES), SP, split_axis=0, concat_...]
    pallas_call x1, Pallas kernels: 7.66 us -> 6.53 us  [mixer(): pl.pallas_call(local_kernel, out_shape=(pltpu.VMEM((T, 4 * LANES), F32),...]
  transfers between devices with their start and end apart: 3 -> 3, of which waited for: 3 -> 3; matrix products, arithmetic and copies ran while one was open for 0% -> 0% of each run, Pallas kernels for 8% -> 7%
where the time goes in v3:
time: 95.7 us; the launch traced here: 95.3 us
  Pallas kernels  27.9 us (29%)
  waiting for transfers between devices  25.8 us (27%)
  blocking collectives  22.7 us (24%)
  starting transfers between devices  18.6 us (19%)
    all_to_all x1, blocking collectives, local(): lax.all_to_all(x.reshape(experts, 8, width // 4), SP_TP, split_axis=0, co...  22.7 us
    all_to_all x1, waiting for transfers between devices, local(): lax.all_to_all(x.reshape(experts, 8, width // 4), SP_TP, split_axis=0, co...  19.2 us
    all_to_all x1, starting transfers between devices, mixer(): lax.all_to_all(send.reshape(blocks, 32, LANES), SP, split_axis=0, concat_...  12 us
    pallas_call x1, Pallas kernels, local(): pl.pallas_call(experts_kernel, out_shape=jax.ShapeDtypeStruct((experts *...  9.25 us
    pallas_call x1, Pallas kernels, mixer(): pl.pallas_call(local_kernel, out_shape=(pltpu.VMEM((T, 4 * LANES), F32),...  6.53 us
    all_to_all x1, waiting for transfers between devices, mixer(): lax.all_to_all(send.reshape(blocks, 32, LANES), SP, split_axis=0, concat_...  5.63 us
    pallas_call x1, Pallas kernels, mixer(): pl.pallas_call(ends_kernel, out_shape=jax.ShapeDtypeStruct((blocks * 32,...  5.51 us
    all_to_all x1, starting transfers between devices, local(): lax.all_to_all(x.reshape(experts, 8, width // 4), SP_TP, split_axis=0, co...  4.43 us
  transfers between devices with their start and end apart: 3, of which 3 were waited for; matrix products, arithmetic and copies ran while one was open for 0% of the time, Pallas kernels for 7%

profile of v3, /device:TPU:1, one launch (start us, length us, event | category | flops | bytes accessed | tf_op | source)
XLA Modules:
  0.0 95.3 jit_solution(5469305802667484543)
XLA Ops:
  0.0 5.5 %ends.1.refs_10_ = bf16[2048,128]{1,0:T(8,128)(2,1)} custom-call(s32[1]{0:T(128)} %bitcast.1.me_ref, bf16[128,256]{1,0:T(8,128)(2,1)} %refs_0_.5, bf16[128,256]{1,0:T(8,128)(2,1)} %refs_1_.5, f32[2,2,16,64]{3,2,1,0:T(8,128)} %refs_2_.4, f32[2,2,16,32]{3,2,1,0:T(8,128)} %refs_3_.4, f32[2,2,16,16,64]{4,3,2,1,0:T(8,128)} %refs_4_.4, ...), custom_call_target="tpu_custom_call" | custom-call | flops 6000000000 | bytes 6000000 | tf_op jit(solution)/shard_map/ends/pallas_call | solution.py:350
  5.5 12.0 %all-to-all-start = ((bf16[64,32,128]{2,1,0:T(8,128)(2,1)}), bf16[64,32,128]{2,1,0:T(8,128)(2,1)S(1)}, u32[]{:S(2)}, u32[]{:S(2)}) async-start(bf16[64,32,128]{2,1,0:T(8,128)(2,1)} %bitcast.3), calls=%async_computation | async-start | bytes 1048576 | tf_op jit(solution)/shard_map/all_to_all | solution.py:360
  17.5 6.5 %local.1 = (f32[128,512]{1,0:T(8,128)S(1)}, bf16[128,6144]{1,0:T(8,128)(2,1)S(1)}, f32[64,128]{1,0:T(8,128)S(1)}) custom-call(bf16[128,256]{1,0:T(8,128)(2,1)} %refs_0_.5, bf16[128,256]{1,0:T(8,128)(2,1)} %refs_1_.5, f32[2,2,16,64]{3,2,1,0:T(8,128)} %refs_2_.4, f32[2,2,16,32]{3,2,1,0:T(8,128)} %refs_3_.4, f32[2,2,16,16,64]{4,3,2,1,0:T(8,128)} %refs_4_.4, ...), custom_call_target="tpu_custom_call" | custom-call | flops 8000000000 | bytes 8000000 | tf_op jit(solution)/shard_map/local/pallas_call | solution.py:364
  24.0 5.6 %all-to-all-done = bf16[64,32,128]{2,1,0:T(8,128)(2,1)S(1)} async-done(((bf16[64,32,128]{2,1,0:T(8,128)(2,1)}), bf16[64,32,128]{2,1,0:T(8,128)(2,1)S(1)}, u32[]{:S(2)}, u32[]{:S(2)}) %all-to-all-start) | async-done | bytes 524320 | tf_op jit(solution)/shard_map/all_to_all | solution.py:360
  29.7 0.0 copy-start
  29.7 0.0 copy-start.1
  29.7 0.0 copy-start.2
  29.7 0.0 copy-start.3
  29.7 0.0 slice-start
  29.7 0.0 slice-start.2
  29.7 3.5 %carry.1 = (bf16[128,512]{1,0:T(8,128)(2,1)S(1)}, bf16[1024,2048]{1,0:T(8,128)(2,1)S(1)}) custom-call(s32[1]{0:T(128)} %bitcast.1.me_ref, bf16[2048,128]{1,0:T(8,128)(2,1)S(1)} %bitcast.24, f32[128,512]{1,0:T(8,128)S(1)} %get-tuple-element.13.y_ref, bf16[128,6144]{1,0:T(8,128)(2,1)S(1)} %get-tuple-element.14.decay_ref, ...), custom_call_target="tpu_custom_call" | custom-call | flops 5000000000 | bytes 5000000 | tf_op jit(solution)/shard_map/carry/pallas_call | solution.py:381
  33.3 2.2 %collective-permute-start = (bf16[64,512]{1,0:T(8,128)(2,1)S(1)}, bf16[64,512]{1,0:T(8,128)(2,1)S(1)}, u32[]{:S(2)}, u32[]{:S(2)}) collective-permute-start(bf16[64,512]{1,0:T(8,128)(2,1)S(1)} %get-tuple-element.21), channel_id=1, source_target_pairs={{0,1},{1,0},{2,3},{3,2},{4,5},{5,4},{6,7},{7,6},{8,9},{9,8},{10,11... | collective-permute-start | bytes 196616 | tf_op jit(solution)/shard_map/ppermute | solution.py:534
  35.5 0.9 collective-permute-done.other_ref
  36.4 0.0 copy-done
  36.4 0.0 copy-done.1
  36.4 0.0 copy-done.2
  36.4 0.0 copy-done.3
  36.4 0.0 slice-start.1
  36.4 0.0 slice-start.3
  36.4 1.6 %project.1 = (bf16[64,2048]{1,0:T(8,128)(2,1)S(1)}, bf16[1024,512]{1,0:T(8,128)(2,1)S(1)}, s32[256,128]{1,0:T(8,128)S(1)}) custom-call(s32[1]{0:T(128)} %bitcast.core_ref, bf16[64,512]{1,0:T(8,128)(2,1)S(1)} %get-tuple-element.22.mine_ref, bf16[64,512]{1,0:T(8,128)(2,1)S(1)} %collective-permute-done.other_ref, s32[2,64]{1,0:T(2,128)S(1)} %bitcast.34, ...), custom_call_target="tpu_custom_call" | custom-call | flops 60000002048 | bytes 60000000 | tf_op jit(solution)/shard_map/project/pallas_call | solution.py:536
  38.1 22.7 %all_to_all.15 = bf16[128,8,512]{2,1,0:T(8,128)(2,1)S(1)} all-to-all(bf16[128,8,512]{2,1,0:T(8,128)(2,1)S(1)} %bitcast.22), channel_id=1, replica_groups=mesh['sp_0'=4,'sp_1'=4,'sp_2'=4,'tp'=2] {'sp_0','sp_1','sp_2','tp'}, dimensions={0} | all-to-all | bytes 2097152 | tf_op jit(solution)/shard_map/all_to_all | solution.py:552
  60.8 0.0 slice-done
  60.8 0.0 slice-done.2
  60.8 0.0 slice-done.1
  60.8 0.0 slice-done.3
  60.8 0.0 copy-start.4
  60.8 9.2 %experts.1 = bf16[1024,512]{1,0:T(8,128)(2,1)} custom-call(bf16[1024,512]{1,0:T(8,128)(2,1)S(1)} %bitcast.23, bf16[2048,1408]{1,0:T(8,128)(2,1)S(1)} %bitcast.28, bf16[2048,1408]{1,0:T(8,128)(2,1)S(1)} %bitcast.31, bf16[1408,2048]{1,0:T(8,128)(2,1)} %bitcast.35), custom_call_target="tpu_custom_call" | custom-call | flops 8999999488 | bytes 9000000 | tf_op jit(solution)/shard_map/experts/pallas_call | solution.py:555
  70.1 4.4 %all-to-all-start.2 = ((bf16[128,8,512]{2,1,0:T(8,128)(2,1)}), bf16[128,8,512]{2,1,0:T(8,128)(2,1)S(1)}, u32[]{:S(2)}, u32[]{:S(2)}) async-start(bf16[128,8,512]{2,1,0:T(8,128)(2,1)} %bitcast.17), calls=%async_computation.2 | async-start | bytes 2097152 | tf_op jit(solution)/shard_map/all_to_all | solution.py:552
  74.5 0.0 copy-done.4
  74.5 0.1 copy.22.weights_ref
  74.6 19.2 %all-to-all-done.2 = bf16[128,8,512]{2,1,0:T(8,128)(2,1)S(1)} async-done(((bf16[128,8,512]{2,1,0:T(8,128)(2,1)}), bf16[128,8,512]{2,1,0:T(8,128)(2,1)S(1)}, u32[]{:S(2)}, u32[]{:S(2)}) %all-to-all-start.2) | async-done | bytes 1048608 | tf_op jit(solution)/shard_map/all_to_all | solution.py:552
  93.9 1.5 %combine.1 = bf16[64,2048]{1,0:T(8,128)(2,1)} custom-call(bf16[1024,512]{1,0:T(8,128)(2,1)S(1)} %bitcast.21, s32[256,128]{1,0:T(8,128)S(1)} %get-tuple-element.19.cols_ref, f32[64,2]{1,0:T(8,128)S(1)} %copy.22.weights_ref, bf16[64,2048]{1,0:T(8,128)(2,1)S(1)} %get-tuple-element.20.hidden_ref), custom_call_target="tpu_custom_call" | custom-call | flops 2000000000 | bytes 2000000 | tf_op jit(solution)/shard_map/combine/pallas_call | solution.py:570
  (3 shorter events, 0.0 us)
Async XLA Ops:
  5.5 24.2 %all-to-all-start = ((bf16[64,32,128]{2,1,0:T(8,128)(2,1)}), bf16[64,32,128]{2,1,0:T(8,128)(2,1)S(1)}, u32[]{:S(2)}, u32[]{:S(2)}) async-start(bf16[64,32,128]{2,1,0:T(8,128)(2,1)} %bitcast.3), calls=%async_computation | async-start | bytes 1048576 | tf_op jit(solution)/shard_map/all_to_all | solution.py:360
  29.7 6.7 %copy-start = (bf16[64,2048]{1,0:T(8,128)(2,1)S(1)}, bf16[64,2048]{1,0:T(8,128)(2,1)}, u32[]{:S(2)}) copy-start(bf16[64,2048]{1,0:T(8,128)(2,1)} %residual_ref.1) | copy-start | bytes 786436
  29.7 6.7 %copy-start.1 = (f32[2048]{0:T(1024)S(1)}, f32[2048]{0:T(1024)}, u32[]{:S(2)}) copy-start(f32[2048]{0:T(1024)} %param.36) | copy-start | bytes 24580
  29.7 6.7 %copy-start.2 = (f32[1024]{0:T(1024)S(1)}, f32[1024]{0:T(1024)}, u32[]{:S(2)}) copy-start(f32[1024]{0:T(1024)} %param.34) | copy-start | bytes 12292
  29.7 6.7 %copy-start.3 = (s32[64,2]{0,1:T(2,128)S(1)}, s32[64,2]{0,1:T(2,128)}, u32[]{:S(2)}) copy-start(s32[64,2]{0,1:T(2,128)} %param.37) | copy-start | bytes 1540
  29.7 31.1 %slice-start = ((s8[5767168]{0:T(1024)(128)(4,1)}), s8[1572864]{0:T(1024)(128)(4,1)S(1)}, s32[]{:S(2)}) async-start(s8[5767168]{0:T(1024)(128)(4,1)} %bitcast.26), calls=%async_computation.3 | async-start | bytes 3145728
  29.7 31.1 %slice-start.2 = ((s8[5767168]{0:T(1024)(128)(4,1)}), s8[4194304]{0:T(1024)(128)(4,1)S(1)}, s32[]{:S(2)}) async-start(s8[5767168]{0:T(1024)(128)(4,1)} %bitcast.29), calls=%async_computation.5 | async-start | bytes 8388608
  33.3 3.1 %collective-permute-start = (bf16[64,512]{1,0:T(8,128)(2,1)S(1)}, bf16[64,512]{1,0:T(8,128)(2,1)S(1)}, u32[]{:S(2)}, u32[]{:S(2)}) collective-permute-start(bf16[64,512]{1,0:T(8,128)(2,1)S(1)} %get-tuple-element.21), channel_id=1, source_target_pairs={{0,1},{1,0},{2,3},{3,2},{4,5},{5,4},{6,7},{7,6},{8,9},{9,8},{10,11... | collective-permute-start | bytes 196616 | tf_op jit(solution)/shard_map/ppermute | solution.py:534
  36.4 24.4 %slice-start.1 = ((s8[5767168]{0:T(1024)(128)(4,1)}), s8[4194304]{0:T(1024)(128)(4,1)S(1)}, s32[]{:S(2)}) async-start(s8[5767168]{0:T(1024)(128)(4,1)} %bitcast.26), calls=%async_computation.4 | async-start | bytes 8388608
  36.4 24.3 %slice-start.3 = ((s8[5767168]{0:T(1024)(128)(4,1)}), s8[1572864]{0:T(1024)(128)(4,1)S(1)}, s32[]{:S(2)}) async-start(s8[5767168]{0:T(1024)(128)(4,1)} %bitcast.29), calls=%async_computation.6 | async-start | bytes 3145728
  60.8 13.7 %copy-start.4 = (f32[64,2]{0,1:T(2,128)S(1)}, f32[64,2]{0,1:T(2,128)}, u32[]{:S(2)}) copy-start(f32[64,2]{0,1:T(2,128)} %param.38) | copy-start | bytes 1540
  70.1 23.8 %all-to-all-start.2 = ((bf16[128,8,512]{2,1,0:T(8,128)(2,1)}), bf16[128,8,512]{2,1,0:T(8,128)(2,1)S(1)}, u32[]{:S(2)}, u32[]{:S(2)}) async-start(bf16[128,8,512]{2,1,0:T(8,128)(2,1)} %bitcast.17), calls=%async_computation.2 | async-start | bytes 2097152 | tf_op jit(solution)/shard_map/all_to_all | solution.py:552

commit v4 on v3

--- a/solution.py
+++ b/solution.py
@@ -142,7 +142,8 @@
 
 
 def ends_kernel(me_ref, *refs):
-    sources, send_ref, buffers, sems, scr = refs[:8], refs[8], refs[9:17], refs[17], refs[18:]
+    sources, send_ref, buffers, sems, scr = refs[:8], refs[8], refs[9:17], refs[17], refs[18:30]
+    blocks_ref = refs[30]
     turns, forget_t = load_pushes(started(sources, buffers, sems), buffers, scr)
 
     def step(t, state):
@@ -174,13 +175,15 @@
         nr = jnp.where(row < 4, nr, jnp.where(row == 4, terms, jnp.where(row == 5, rest, 0.0)))
         blocks.append(jnp.concatenate([wr, wi, nr, jnp.where(row < 4, ni, 0.0)], axis=0))
     me = me_ref[0]
+    blocks_ref[...] = jnp.concatenate(blocks, axis=0).astype(BF16)
 
     def put(j, _):
         at = pl.multiple_of(j * 32, 32)
-        send_ref[pl.ds(at, 32), :] = jnp.where(j > me, blocks[0], blocks[1]).astype(BF16)
+        start = pl.multiple_of(jnp.where(j > me, 0, 32), 32)
+        send_ref[pl.ds(at, 32), :] = blocks_ref[pl.ds(start, 32), :]
         return 0
 
-    lax.fori_loop(0, send_ref.shape[0] // 32, put, 0)
+    lax.fori_loop(0, send_ref.shape[0] // 32, put, 0, unroll=8)
 
 
 def read_blocks(out_ref, d, r, kind):
@@ -352,7 +355,7 @@
         out_shape=jax.ShapeDtypeStruct((blocks * 32, LANES), BF16),
         in_specs=[SMEM] + [HBM] * 8,
         out_specs=VMEM,
-        scratch_shapes=fetched(shared) + [column(T)] * 12,
+        scratch_shapes=fetched(shared) + [column(T)] * 12 + [pltpu.VMEM((64, LANES), BF16)],
         compiler_params=grant(20),
         cost_estimate=cost(6),
         name="ends",
@@ -462,10 +465,8 @@
 
 
 def experts_kernel(
-    in_ref, gate_ref, up_ref, far_ref, out_ref, x_ref, h_ref, down_ref, sem
+    in_ref, gate_ref, up_ref, down_ref, out_ref, x_ref, h_ref
 ):
-    copy = pltpu.make_async_copy(far_ref, down_ref, sem)
-    copy.start()
     quarter = in_ref.shape[1]
     turn = turned(False)
     for b in range(4):
@@ -480,7 +481,6 @@
     gate = jnp.dot(x, gate_ref[...], preferred_element_type=F32)
     up = jnp.dot(x, up_ref[...], preferred_element_type=F32)
     h_ref[...] = (gate * jax.nn.sigmoid(gate) * up).astype(BF16)
-    copy.wait()
     done = jnp.dot(h_ref[...], down_ref[...], preferred_element_type=F32).astype(BF16)
     back = turned(True)
     for b in range(4):
@@ -555,18 +555,16 @@
     done = pl.pallas_call(
         experts_kernel,
         out_shape=jax.ShapeDtypeStruct((experts * 8, width // 4), BF16),
-        in_specs=[VMEM] * 3 + [HBM],
+        in_specs=[VMEM] * 4,
         out_specs=VMEM,
         scratch_shapes=[
             pltpu.VMEM((2 * experts, width), BF16),
             pltpu.VMEM((2 * experts, gate_proj.shape[2]), BF16),
-            pltpu.VMEM(down_proj.shape[1:], BF16),
-            pltpu.SemaphoreType.DMA,
         ],
-        compiler_params=grant(20),
+        compiler_params=grant(12),
         cost_estimate=cost(9),
         name="experts",
-    )(exchange(send), gate_proj[0], up_proj[0], *far((down_proj[0],)))
+    )(exchange(send), gate_proj[0], up_proj[0], down_proj[0])
     return pl.pallas_call(
         combine_kernel,
         out_shape=jax.ShapeDtypeStruct((rows, width), BF16),

time: 95.7 us -> 93 us (0.972)
  Pallas kernels: 27.9 us -> 25.2 us
    pallas_call x1, Pallas kernels: 9.25 us -> 6.83 us  [local(): pl.pallas_call(experts_kernel, out_shape=jax.ShapeDtypeStruct((experts *...]
where the time goes in v4:
time: 93 us; the launch traced here: 92.7 us
  waiting for transfers between devices  25.8 us (28%)
  Pallas kernels  25.2 us (27%)
  blocking collectives  22.7 us (24%)
  starting transfers between devices  18.6 us (20%)
    all_to_all x1, blocking collectives, local(): lax.all_to_all(x.reshape(experts, 8, width // 4), SP_TP, split_axis=0, co...  22.7 us
    all_to_all x1, waiting for transfers between devices, local(): lax.all_to_all(x.reshape(experts, 8, width // 4), SP_TP, split_axis=0, co...  19.2 us
    all_to_all x1, starting transfers between devices, mixer(): lax.all_to_all(send.reshape(blocks, 32, LANES), SP, split_axis=0, concat_...  12 us
    pallas_call x1, Pallas kernels, local(): pl.pallas_call(experts_kernel, out_shape=jax.ShapeDtypeStruct((experts *...  6.83 us
    pallas_call x1, Pallas kernels, mixer(): pl.pallas_call(local_kernel, out_shape=(pltpu.VMEM((T, 4 * LANES), F32),...  6.53 us
    all_to_all x1, waiting for transfers between devices, mixer(): lax.all_to_all(send.reshape(blocks, 32, LANES), SP, split_axis=0, concat_...  5.64 us
    pallas_call x1, Pallas kernels, mixer(): pl.pallas_call(ends_kernel, out_shape=jax.ShapeDtypeStruct((blocks * 32,...  5.29 us
    all_to_all x1, starting transfers between devices, local(): lax.all_to_all(x.reshape(experts, 8, width // 4), SP_TP, split_axis=0, co...  4.42 us
  transfers between devices with their start and end apart: 3, of which 3 were waited for; matrix products, arithmetic and copies ran while one was open for 0% of the time, Pallas kernels for 7%

profile of v4, /device:TPU:1, one launch (start us, length us, event | category | flops | bytes accessed | tf_op | source)
XLA Modules:
  0.0 92.7 jit_solution(13689939734083572135)
XLA Ops:
  0.0 5.3 %ends.1.refs_10_ = bf16[2048,128]{1,0:T(8,128)(2,1)} custom-call(s32[1]{0:T(128)} %bitcast.1.me_ref, bf16[128,256]{1,0:T(8,128)(2,1)} %refs_0_.5, bf16[128,256]{1,0:T(8,128)(2,1)} %refs_1_.5, f32[2,2,16,64]{3,2,1,0:T(8,128)} %refs_2_.4, f32[2,2,16,32]{3,2,1,0:T(8,128)} %refs_3_.4, f32[2,2,16,16,64]{4,3,2,1,0:T(8,128)} %refs_4_.4, ...), custom_call_target="tpu_custom_call" | custom-call | flops 6000000000 | bytes 6000000 | tf_op jit(solution)/shard_map/ends/pallas_call | solution.py:353
  5.3 12.0 %all-to-all-start = ((bf16[64,32,128]{2,1,0:T(8,128)(2,1)}), bf16[64,32,128]{2,1,0:T(8,128)(2,1)S(1)}, u32[]{:S(2)}, u32[]{:S(2)}) async-start(bf16[64,32,128]{2,1,0:T(8,128)(2,1)} %bitcast.3), calls=%async_computation | async-start | bytes 1048576 | tf_op jit(solution)/shard_map/all_to_all | solution.py:363
  17.3 6.5 %local.1 = (f32[128,512]{1,0:T(8,128)S(1)}, bf16[128,6144]{1,0:T(8,128)(2,1)S(1)}, f32[64,128]{1,0:T(8,128)S(1)}) custom-call(bf16[128,256]{1,0:T(8,128)(2,1)} %refs_0_.5, bf16[128,256]{1,0:T(8,128)(2,1)} %refs_1_.5, f32[2,2,16,64]{3,2,1,0:T(8,128)} %refs_2_.4, f32[2,2,16,32]{3,2,1,0:T(8,128)} %refs_3_.4, f32[2,2,16,16,64]{4,3,2,1,0:T(8,128)} %refs_4_.4, ...), custom_call_target="tpu_custom_call" | custom-call | flops 8000000000 | bytes 8000000 | tf_op jit(solution)/shard_map/local/pallas_call | solution.py:367
  23.8 5.6 %all-to-all-done = bf16[64,32,128]{2,1,0:T(8,128)(2,1)S(1)} async-done(((bf16[64,32,128]{2,1,0:T(8,128)(2,1)}), bf16[64,32,128]{2,1,0:T(8,128)(2,1)S(1)}, u32[]{:S(2)}, u32[]{:S(2)}) %all-to-all-start) | async-done | bytes 524320 | tf_op jit(solution)/shard_map/all_to_all | solution.py:363
  29.5 0.0 copy-start
  29.5 0.0 copy-start.1
  29.5 0.0 copy-start.2
  29.5 0.0 copy-start.3
  29.5 0.0 slice-start
  29.5 0.0 slice-start.2
  29.5 0.0 slice-start.4
  29.5 3.5 %carry.1 = (bf16[128,512]{1,0:T(8,128)(2,1)S(1)}, bf16[1024,2048]{1,0:T(8,128)(2,1)S(1)}) custom-call(s32[1]{0:T(128)} %bitcast.1.me_ref, bf16[2048,128]{1,0:T(8,128)(2,1)S(1)} %bitcast.24, f32[128,512]{1,0:T(8,128)S(1)} %get-tuple-element.13.y_ref, bf16[128,6144]{1,0:T(8,128)(2,1)S(1)} %get-tuple-element.14.decay_ref, ...), custom_call_target="tpu_custom_call" | custom-call | flops 5000000000 | bytes 5000000 | tf_op jit(solution)/shard_map/carry/pallas_call | solution.py:384
  33.1 2.2 %collective-permute-start = (bf16[64,512]{1,0:T(8,128)(2,1)S(1)}, bf16[64,512]{1,0:T(8,128)(2,1)S(1)}, u32[]{:S(2)}, u32[]{:S(2)}) collective-permute-start(bf16[64,512]{1,0:T(8,128)(2,1)S(1)} %get-tuple-element.21), channel_id=1, source_target_pairs={{0,1},{1,0},{2,3},{3,2},{4,5},{5,4},{6,7},{7,6},{8,9},{9,8},{10,11... | collective-permute-start | bytes 196616 | tf_op jit(solution)/shard_map/ppermute | solution.py:534
  35.3 0.9 collective-permute-done.other_ref
  36.2 0.0 copy-done
  36.2 0.0 copy-done.1
  36.2 0.0 copy-done.2
  36.2 0.0 copy-done.3
  36.2 0.0 slice-start.1
  36.2 0.0 slice-start.3
  36.2 0.0 slice-start.5
  36.3 1.6 %project.1 = (bf16[64,2048]{1,0:T(8,128)(2,1)S(1)}, bf16[1024,512]{1,0:T(8,128)(2,1)S(1)}, s32[256,128]{1,0:T(8,128)S(1)}) custom-call(s32[1]{0:T(128)} %bitcast.core_ref, bf16[64,512]{1,0:T(8,128)(2,1)S(1)} %get-tuple-element.22.mine_ref, bf16[64,512]{1,0:T(8,128)(2,1)S(1)} %collective-permute-done.other_ref, s32[2,64]{1,0:T(2,128)S(1)} %bitcast.37, ...), custom_call_target="tpu_custom_call" | custom-call | flops 60000002048 | bytes 60000000 | tf_op jit(solution)/shard_map/project/pallas_call | solution.py:536
  37.9 22.7 %all_to_all.15 = bf16[128,8,512]{2,1,0:T(8,128)(2,1)S(1)} all-to-all(bf16[128,8,512]{2,1,0:T(8,128)(2,1)S(1)} %bitcast.22), channel_id=1, replica_groups=mesh['sp_0'=4,'sp_1'=4,'sp_2'=4,'tp'=2] {'sp_0','sp_1','sp_2','tp'}, dimensions={0} | all-to-all | bytes 2097152 | tf_op jit(solution)/shard_map/all_to_all | solution.py:552
  60.6 0.0 slice-done
  60.6 0.0 slice-done.2
  60.6 0.0 slice-done.4
  60.6 0.0 slice-done.1
  60.6 0.0 slice-done.3
  60.6 0.0 slice-done.5
  60.6 0.0 copy-start.4
  60.7 6.8 %experts.1 = bf16[1024,512]{1,0:T(8,128)(2,1)} custom-call(bf16[1024,512]{1,0:T(8,128)(2,1)S(1)} %bitcast.23, bf16[2048,1408]{1,0:T(8,128)(2,1)S(1)} %bitcast.28, bf16[2048,1408]{1,0:T(8,128)(2,1)S(1)} %bitcast.31, bf16[1408,2048]{1,0:T(8,128)(2,1)S(1)} %bitcast.34), custom_call_target="tpu_custom_call" | custom-call | flops 8999999488 | bytes 9000000 | tf_op jit(solution)/shard_map/experts/pallas_call | solution.py:555
  67.5 4.4 %all-to-all-start.2 = ((bf16[128,8,512]{2,1,0:T(8,128)(2,1)}), bf16[128,8,512]{2,1,0:T(8,128)(2,1)S(1)}, u32[]{:S(2)}, u32[]{:S(2)}) async-start(bf16[128,8,512]{2,1,0:T(8,128)(2,1)} %bitcast.17), calls=%async_computation.2 | async-start | bytes 2097152 | tf_op jit(solution)/shard_map/all_to_all | solution.py:552
  71.9 0.0 copy-done.4
  71.9 0.1 copy.22.weights_ref
  72.0 19.2 %all-to-all-done.2 = bf16[128,8,512]{2,1,0:T(8,128)(2,1)S(1)} async-done(((bf16[128,8,512]{2,1,0:T(8,128)(2,1)}), bf16[128,8,512]{2,1,0:T(8,128)(2,1)S(1)}, u32[]{:S(2)}, u32[]{:S(2)}) %all-to-all-start.2) | async-done | bytes 1048608 | tf_op jit(solution)/shard_map/all_to_all | solution.py:552
  91.2 1.5 %combine.1 = bf16[64,2048]{1,0:T(8,128)(2,1)} custom-call(bf16[1024,512]{1,0:T(8,128)(2,1)S(1)} %bitcast.21, s32[256,128]{1,0:T(8,128)S(1)} %get-tuple-element.19.cols_ref, f32[64,2]{1,0:T(8,128)S(1)} %copy.22.weights_ref, bf16[64,2048]{1,0:T(8,128)(2,1)S(1)} %get-tuple-element.20.hidden_ref), custom_call_target="tpu_custom_call" | custom-call | flops 2000000000 | bytes 2000000 | tf_op jit(solution)/shard_map/combine/pallas_call | solution.py:568
  (4 shorter events, 0.0 us)
Async XLA Ops:
  5.3 24.2 %all-to-all-start = ((bf16[64,32,128]{2,1,0:T(8,128)(2,1)}), bf16[64,32,128]{2,1,0:T(8,128)(2,1)S(1)}, u32[]{:S(2)}, u32[]{:S(2)}) async-start(bf16[64,32,128]{2,1,0:T(8,128)(2,1)} %bitcast.3), calls=%async_computation | async-start | bytes 1048576 | tf_op jit(solution)/shard_map/all_to_all | solution.py:363
  29.5 6.7 %copy-start = (bf16[64,2048]{1,0:T(8,128)(2,1)S(1)}, bf16[64,2048]{1,0:T(8,128)(2,1)}, u32[]{:S(2)}) copy-start(bf16[64,2048]{1,0:T(8,128)(2,1)} %residual_ref.1) | copy-start | bytes 786436
  29.5 6.7 %copy-start.1 = (f32[2048]{0:T(1024)S(1)}, f32[2048]{0:T(1024)}, u32[]{:S(2)}) copy-start(f32[2048]{0:T(1024)} %param.36) | copy-start | bytes 24580
  29.5 6.7 %copy-start.2 = (f32[1024]{0:T(1024)S(1)}, f32[1024]{0:T(1024)}, u32[]{:S(2)}) copy-start(f32[1024]{0:T(1024)} %param.34) | copy-start | bytes 12292
  29.5 6.7 %copy-start.3 = (s32[64,2]{0,1:T(2,128)S(1)}, s32[64,2]{0,1:T(2,128)}, u32[]{:S(2)}) copy-start(s32[64,2]{0,1:T(2,128)} %param.37) | copy-start | bytes 1540
  29.5 31.1 %slice-start = ((s8[5767168]{0:T(1024)(128)(4,1)}), s8[4194304]{0:T(1024)(128)(4,1)S(1)}, s32[]{:S(2)}) async-start(s8[5767168]{0:T(1024)(128)(4,1)} %bitcast.26), calls=%async_computation.3 | async-start | bytes 8388608
  29.5 31.1 %slice-start.2 = ((s8[5767168]{0:T(1024)(128)(4,1)}), s8[1572864]{0:T(1024)(128)(4,1)S(1)}, s32[]{:S(2)}) async-start(s8[5767168]{0:T(1024)(128)(4,1)} %bitcast.29), calls=%async_computation.5 | async-start | bytes 3145728
  29.5 31.1 %slice-start.4 = ((s8[5767168]{0:T(1024)(128)(4,1)}), s8[4194304]{0:T(1024)(128)(4,1)S(1)}, s32[]{:S(2)}) async-start(s8[5767168]{0:T(1024)(128)(4,1)} %bitcast.32), calls=%async_computation.7 | async-start | bytes 8388608
  33.1 3.1 %collective-permute-start = (bf16[64,512]{1,0:T(8,128)(2,1)S(1)}, bf16[64,512]{1,0:T(8,128)(2,1)S(1)}, u32[]{:S(2)}, u32[]{:S(2)}) collective-permute-start(bf16[64,512]{1,0:T(8,128)(2,1)S(1)} %get-tuple-element.21), channel_id=1, source_target_pairs={{0,1},{1,0},{2,3},{3,2},{4,5},{5,4},{6,7},{7,6},{8,9},{9,8},{10,11... | collective-permute-start | bytes 196616 | tf_op jit(solution)/shard_map/ppermute | solution.py:534
  36.2 24.4 %slice-start.1 = ((s8[5767168]{0:T(1024)(128)(4,1)}), s8[1572864]{0:T(1024)(128)(4,1)S(1)}, s32[]{:S(2)}) async-start(s8[5767168]{0:T(1024)(128)(4,1)} %bitcast.26), calls=%async_computation.4 | async-start | bytes 3145728
  36.2 24.4 %slice-start.3 = ((s8[5767168]{0:T(1024)(128)(4,1)}), s8[4194304]{0:T(1024)(128)(4,1)S(1)}, s32[]{:S(2)}) async-start(s8[5767168]{0:T(1024)(128)(4,1)} %bitcast.29), calls=%async_computation.6 | async-start | bytes 8388608
  36.2 24.4 %slice-start.5 = ((s8[5767168]{0:T(1024)(128)(4,1)}), s8[1572864]{0:T(1024)(128)(4,1)S(1)}, s32[]{:S(2)}) async-start(s8[5767168]{0:T(1024)(128)(4,1)} %bitcast.32), calls=%async_computation.8 | async-start | bytes 3145728
  60.6 11.3 %copy-start.4 = (f32[64,2]{0,1:T(2,128)S(1)}, f32[64,2]{0,1:T(2,128)}, u32[]{:S(2)}) copy-start(f32[64,2]{0,1:T(2,128)} %param.38) | copy-start | bytes 1540
  67.5 23.8 %all-to-all-start.2 = ((bf16[128,8,512]{2,1,0:T(8,128)(2,1)}), bf16[128,8,512]{2,1,0:T(8,128)(2,1)S(1)}, u32[]{:S(2)}, u32[]{:S(2)}) async-start(bf16[128,8,512]{2,1,0:T(8,128)(2,1)} %bitcast.17), calls=%async_computation.2 | async-start | bytes 2097152 | tf_op jit(solution)/shard_map/all_to_all | solution.py:552
